TPU v7x, 256 devices: a whole 4x4x8 slice. The times are simulated.
256 devices in a mesh: ep: 64 (over z, y, core), tp: 4 (over x).
Axes of the slice: x: 4, y: 4, z: 8, core: 2. Of those that a mesh axis runs over, the one named last changes fastest.
Arguments:
- tokens: bfloat16 [1024, 2048], P('ep'), may hold values from -6 to 6
- lengths: int32 [1024], P('ep'), may hold values from 256 to 1023
- cache: bfloat16 [1024, 1024, 512], P('ep', None, 'tp'), may hold values from -6 to 6
- attn_gain: float32 [2048], replicated, may hold values from 0.1 to 1.9
- query_weight: bfloat16 [2048, 1024], P(None, 'tp'), may hold values from -0.125 to 0.125
- key_weight: bfloat16 [2048, 256], P(None, 'tp'), may hold values from -0.125 to 0.125
- value_weight: bfloat16 [2048, 256], P(None, 'tp'), may hold values from -0.125 to 0.125
- stick_bias: float32 [16], P('tp'), may hold values from -7 to -1
- out_weight: bfloat16 [1024, 2048], P('tp'), may hold values from -0.1875 to 0.1875
- ffn_gain: float32 [2048], replicated, may hold values from 0.1 to 1.9
- routes: int32 [1024, 6], P('ep'), may hold values from 0 to 63, all different within a row; in each aligned block of 16 rows (0 to 15, 16 to 31, ...) at most 3 rows name the same one
- route_weights: float32 [1024, 6], P('ep'), may hold values from 0.1 to 0.6
- expert_gate: bfloat16 [64, 2048, 1024], P('ep', None, 'tp'), may hold values from -0.125 to 0.125
- expert_up: bfloat16 [64, 2048, 1024], P('ep', None, 'tp'), may hold values from -0.125 to 0.125
- expert_down: bfloat16 [64, 1024, 2048], P('ep', 'tp'), may hold values from -0.1875 to 0.1875
- shared_gate: bfloat16 [2048, 512], P('ep', 'tp'), may hold values from -0.125 to 0.125
- shared_up: bfloat16 [2048, 512], P('ep', 'tp'), may hold values from -0.125 to 0.125
- shared_down: bfloat16 [512, 2048], P('tp'), may hold values from -0.25 to 0.25
- gate_vector: bfloat16 [2048], replicated, may hold values from -0.125 to 0.125
Outputs:
- layer_out: bfloat16 [1024, 2048], P('ep', 'tp')
- new_kv: bfloat16 [1024, 512], P('ep', 'tp')
Inputs may be any that keep to these rules, and one draw needn't show every extreme that they name: Each sequence's new token comes after its lengths cached positions. `routes`: each row names 6 different experts; among the 16 rows of one index of ep no expert is named by more than 3 rows.
All inputs are finite; a program needn't handle non-finite values.
Results may differ from a plain program's by a relative error of at most 0.012.
Values may be sent and summed in bfloat16 or wider, within the bound.
A program may use at most 64 MiB of HBM per device.

v0:
```python
import jax
import jax.numpy as jnp
from jax import lax
from jax.sharding import PartitionSpec as P

HEAD_DIM = 64


epsilon = 1e-06


def copy_for_each(array, axis):
    copies = jnp.broadcast_to(array, (lax.axis_size(axis), *array.shape))
    return lax.all_to_all(copies, axis, split_axis=0, concat_axis=0, tiled=True)


def of_everyone(array, axis):
    return copy_for_each(array, axis).astype(jnp.float32).sum(axis=0)


def split_up(array, dim, length):
    before, after = (array.shape[:dim], array.shape[dim + 1 :])
    return jnp.moveaxis(array.reshape(*before, length, -1, *after), dim, 0)


def sent_and_summed(array, axis, dim):
    parts = split_up(array, dim, lax.axis_size(axis))
    arrived = lax.all_to_all(parts, axis, split_axis=0, concat_axis=0, tiled=True)
    return arrived.astype(jnp.float32).sum(axis=0)


def side_by_side(arrays, axis, dim, along):
    ends, at = ([], 0)
    for a in arrays[:-1]:
        at += a.shape[along]
        ends.append(at)
    both = jnp.concatenate(arrays, axis=along)
    return tuple(jnp.split(sent_and_summed(both, axis, dim), ends, axis=along))


def rms_scale(rows_in, gain_row):
    values_f = rows_in.astype(jnp.float32)
    return (
        values_f
        * lax.rsqrt(jnp.mean(values_f * values_f, axis=-1, keepdims=True) + epsilon)
        * gain_row
    )


def later_sum(values):
    lead = values.shape[:-1]
    length = values.shape[-1]
    width = 128
    count = length // width
    blocked = values.reshape(lead + (count, width))
    inner_rows = lax.broadcasted_iota(jnp.int32, (width, width), 0)
    inner_cols = lax.broadcasted_iota(jnp.int32, (width, width), 1)
    inner_table = (inner_rows > inner_cols).astype(jnp.float32)
    within = jnp.einsum("...bj,js->...bs", blocked, inner_table, precision=lax.Precision.HIGHEST)
    totals = jnp.sum(blocked, axis=-1)
    outer_rows = lax.broadcasted_iota(jnp.int32, (count, count), 0)
    outer_cols = lax.broadcasted_iota(jnp.int32, (count, count), 1)
    outer_table = (outer_rows > outer_cols).astype(jnp.float32)
    beyond = jnp.einsum("...j,ji->...i", totals, outer_table, precision=lax.Precision.HIGHEST)
    return (within + beyond[..., None]).reshape(lead + (length,))


def shards(
    tokens,
    lengths,
    cache,
    attn_gain,
    query_weight,
    key_weight,
    value_weight,
    stick_bias,
    out_weight,
    ffn_gain,
    routes,
    route_weights,
    expert_gate,
    expert_up,
    expert_down,
    shared_gate,
    shared_up,
    shared_down,
    gate_vector,
):
    ranks_tp = lax.axis_size("tp")
    ranks_ep = lax.axis_size("ep")
    row_count = tokens.shape[0]
    model_width = tokens.shape[1]
    quarter = model_width // ranks_tp
    part_index = lax.axis_index("tp")
    normed = rms_scale(tokens, attn_gain).astype(jnp.bfloat16)
    queries = jnp.dot(normed, query_weight, preferred_element_type=jnp.float32).astype(jnp.bfloat16)
    key_rows = jnp.dot(normed, key_weight, preferred_element_type=jnp.float32).astype(jnp.bfloat16)
    value_rows = jnp.dot(normed, value_weight, preferred_element_type=jnp.float32).astype(
        jnp.bfloat16
    )
    local_heads = key_weight.shape[1] // HEAD_DIM
    new_kv = jnp.stack(
        [
            key_rows.reshape(row_count, local_heads, HEAD_DIM),
            value_rows.reshape(row_count, local_heads, HEAD_DIM),
        ],
        axis=2,
    )
    new_kv = new_kv.reshape(row_count, local_heads * 2 * HEAD_DIM)
    group_size = queries.shape[1] // HEAD_DIM // local_heads
    grouped = queries.reshape(row_count, local_heads, group_size, HEAD_DIM)
    cache_len = cache.shape[1]
    cache_view = cache.reshape(row_count, cache_len, local_heads, 2, HEAD_DIM)
    scores = jnp.einsum(
        "nkgd,nckd->nkgc", grouped, cache_view[:, :, :, 0, :], preferred_element_type=jnp.float32
    ) * HEAD_DIM ** (-0.5)
    scores = scores + stick_bias.reshape(1, local_heads, group_size, 1)
    positions = lax.broadcasted_iota(jnp.int32, (1, 1, 1, cache_len), 3)
    usable = positions < lengths.reshape(row_count, 1, 1, 1)
    log_keep = jnp.where(usable, jax.nn.log_sigmoid(-scores), 0.0)
    behind = later_sum(log_keep)
    stick_weights = jnp.where(usable, jnp.exp(jax.nn.log_sigmoid(scores) + behind), 0.0).astype(
        jnp.bfloat16
    )
    heads_out = jnp.einsum(
        "nkgc,nckd->nkgd",
        stick_weights,
        cache_view[:, :, :, 1, :],
        preferred_element_type=jnp.float32,
    ).astype(jnp.bfloat16)
    attn_term = jnp.dot(
        heads_out.reshape(row_count, -1), out_weight, preferred_element_type=jnp.float32
    )
    attn_total = of_everyone(attn_term.astype(jnp.bfloat16), "tp").astype(jnp.float32)
    residual_full = tokens.astype(jnp.float32) + attn_total
    normed_mix = rms_scale(residual_full, ffn_gain).astype(jnp.bfloat16)
    residual = lax.dynamic_slice_in_dim(residual_full, part_index * quarter, quarter, 1)
    route_count = routes.shape[1]
    local_experts = expert_gate.shape[0]
    experts_all = ranks_ep * local_experts
    capacity = min(row_count, max(2, 2 * row_count * route_count // experts_all))
    slot_total = experts_all * capacity
    flat_routes = routes.reshape(-1)
    flat_count = flat_routes.shape[0]
    expert_hits = (
        flat_routes[:, None] == lax.broadcasted_iota(jnp.int32, (1, experts_all), 1)
    ).astype(jnp.float32)
    lower_table = (
        lax.broadcasted_iota(jnp.int32, (flat_count, flat_count), 0)
        > lax.broadcasted_iota(jnp.int32, (flat_count, flat_count), 1)
    ).astype(jnp.float32)
    earlier = jnp.dot(lower_table, expert_hits, precision=lax.Precision.HIGHEST)
    slot_rank = jnp.sum(earlier * expert_hits, axis=1).astype(jnp.int32)
    slot_index = flat_routes * capacity + slot_rank
    owned_slots = slot_index[:, None] == lax.broadcasted_iota(jnp.int32, (1, slot_total), 1)
    owned_slots = owned_slots.reshape(row_count, route_count, slot_total)
    take_matrix = jnp.any(owned_slots, axis=1).astype(jnp.bfloat16)
    mix_weights = jnp.sum(owned_slots.astype(jnp.float32) * route_weights[:, :, None], axis=1)
    pick_dims = (((0,), (0,)), ((), ()))
    sent_rows = lax.dot_general(
        take_matrix, normed_mix, pick_dims, preferred_element_type=jnp.float32
    ).astype(jnp.bfloat16)
    arrived = lax.all_to_all(sent_rows, "ep", split_axis=0, concat_axis=0, tiled=True)
    expert_grid = arrived.reshape(ranks_ep, local_experts, capacity, model_width)
    gate_val = jnp.einsum(
        "sjcd,jdf->sjcf", expert_grid, expert_gate, preferred_element_type=jnp.float32
    )
    up_val = jnp.einsum(
        "sjcd,jdf->sjcf", expert_grid, expert_up, preferred_element_type=jnp.float32
    )
    expert_hidden = (jax.nn.silu(gate_val) * up_val).astype(jnp.bfloat16)
    expert_term = jnp.einsum(
        "sjcf,jfd->sjcd", expert_hidden, expert_down, preferred_element_type=jnp.float32
    )
    expert_term = expert_term.reshape(-1, model_width)
    shared_width = shared_gate.shape[1]
    column_rows = lax.all_to_all(normed_mix, "ep", split_axis=1, concat_axis=0, tiled=True)
    joined_weights = jnp.concatenate([shared_gate, shared_up], axis=1)
    dense_total = sent_and_summed(
        jnp.dot(column_rows, joined_weights, preferred_element_type=jnp.float32).astype(
            jnp.bfloat16
        ),
        "ep",
        0,
    )
    gate_sum = dense_total[:, :shared_width]
    up_sum = dense_total[:, shared_width:]
    shared_hidden = (jax.nn.silu(gate_sum) * up_sum).astype(jnp.bfloat16)
    shared_term = jnp.dot(shared_hidden, shared_down, preferred_element_type=jnp.float32)
    expert_share, shared_share = side_by_side(
        (expert_term.astype(jnp.bfloat16), shared_term.astype(jnp.bfloat16)), "tp", 1, 0
    )
    expert_out = expert_share.astype(jnp.bfloat16).reshape(
        ranks_ep, local_experts * capacity, quarter
    )
    returned = lax.all_to_all(expert_out, "ep", split_axis=0, concat_axis=0, tiled=True).reshape(
        slot_total, quarter
    )
    routed = jnp.dot(mix_weights, returned.astype(jnp.float32), precision=lax.Precision.HIGHEST)
    mix_gate = jax.nn.sigmoid(jnp.dot(normed_mix, gate_vector, preferred_element_type=jnp.float32))
    layer_out = (residual + routed + mix_gate[:, None] * shared_share).astype(jnp.bfloat16)
    return (layer_out, new_kv)


def solution(mesh):
    placed = (
        P("ep", None),
        P("ep"),
        P("ep", None, "tp"),
        P(),
        P(None, "tp"),
        P(None, "tp"),
        P(None, "tp"),
        P("tp"),
        P("tp", None),
        P(),
        P("ep", None),
        P("ep", None),
        P("ep", None, "tp"),
        P("ep", None, "tp"),
        P("ep", "tp", None),
        P("ep", "tp"),
        P("ep", "tp"),
        P("tp", None),
        P(),
    )
    return jax.shard_map(
        shards,
        mesh=mesh,
        in_specs=placed,
        out_specs=(P("ep", "tp"), P("ep", "tp")),
        check_vma=False,
    )
```

profile of v0, /device:TPU:2, one launch (start us, length us, event | category | flops | bytes accessed | tf_op | source)
XLA Modules:
  0.0 151.6 jit_solution(14038592422454993125)
XLA Ops:
  0.6 0.0 copy-start
  0.6 1.1 fusion.39
  1.7 1.6 %convolution_convert_fusion.5 = bf16[16,256]{1,0:T(8,128)(2,1)S(1)} fusion(bf16[2048,256]{1,0:T(8,128)(2,1)} %param.23, bf16[16,2048]{1,0:T(8,128)(2,1)} %param.19, f32[2048]{0:T(1024)} %param.22, f32[16]{0:T(128)S(1)} %add_rsqrt_fusion.1), kind=kOutput, calls=%fused_computation.25 | convolution fusion | flops 16912384 | bytes 1130560 | tf_op jit(solution)/shard_map/dot_general | solution.py:96
  3.3 0.1 reshape.190
  3.4 0.0 copy-start.17
  3.4 6.4 %copy.65 = bf16[16,1024,128]{1,2,0:T(8,128)(2,1)} copy(bf16[16,1024,128]{2,1,0:T(8,128)(2,1)} %param.21) | data formatting | bytes 8388608 | tf_op args[2]
  9.8 0.1 iota_compare_fusion.2
  9.9 2.2 %fusion.32 = (f32[16,4,1024]{2,1,0:T(4,128)S(1)}, f32[16,4,1024]{2,1,0:T(4,128)S(1)}) fusion(pred[16,1024]{1,0:T(8,128)(4,1)S(1)} %iota_compare_fusion.2, f32[4]{0:T(128)S(1)} %copy-done.17, bf16[16,4,64]{2,1,0:T(4,128)(2,1)S(1)} %reshape.190, bf16[16,1024,1,2,64]{1,4,3,0,2:T(8,128)(2,1)} %bitcast.121), kind=kOutput, calls=%fused_computation.53 | convolution fusion | flops 9043968 | bytes 2646032 | tf_op jit(solution)/shard_map/nkgd,nckd->nkgc/dot_general | solution.py:114
  12.1 0.1 reshape.193
  12.2 0.2 reduce_sum.73
  12.4 0.2 fusion.48
  12.6 0.1 copy.68
  12.7 0.3 convolution_add_fusion
  13.0 0.1 reshape.194
  13.1 0.0 copy-start.1
  13.1 2.4 %fusion.10 = bf16[16,4,64]{2,1,0:T(4,128)(2,1)S(1)} fusion(bf16[16,1024,1,2,64]{1,4,3,0,2:T(8,128)(2,1)} %bitcast.122, f32[16,4,1024]{2,1,0:T(4,128)S(1)} %reshape.194, f32[16,4,1024]{2,1,0:T(4,128)S(1)} %get-tuple-element.5, pred[16,1024]{1,0:T(8,128)(4,1)S(1)} %iota_compare_fusion.2), kind=kOutput, calls=%fused_computation.23 | convolution fusion | flops 9113600 | bytes 2646016 | tf_op jit(solution)/shard_map/nkgc,nckd->nkgd/dot_general | solution.py:125
  15.4 0.1 reshape.196
  15.5 0.0 copy-start.9
  15.6 0.2 convolution_convert_fusion.3
  15.8 9.8 %all_to_all.48 = bf16[4,16,2048]{2,1,0:T(8,128)(2,1)S(1)} all-to-all(bf16[4,16,2048]{2,1,0:T(8,128)(2,1)S(1)} %broadcast_in_dim.26), channel_id=1, replica_groups=mesh['ep'=64,'tp'=4] {'tp'}, dimensions={0} | all-to-all | bytes 524288 | tf_op jit(solution)/shard_map/all_to_all | solution.py:14
  25.7 0.0 copy-start.7
  25.7 0.1 multiply_reduce_fusion
  25.9 0.1 multiply_convert_fusion
  26.0 0.2 all_to_all.35
  26.2 0.2 copy.92
  26.4 0.2 reshape.213
  26.5 21.9 %all_to_all.49 = bf16[64,2,256]{2,1,0:T(2,128)(2,1)S(1)} all-to-all(bf16[64,2,256]{2,1,0:T(2,128)(2,1)S(1)} %reshape.213), channel_id=1, replica_groups=mesh['ep'=64,'tp'=4] {'ep'}, dimensions={0} | all-to-all | bytes 131072 | tf_op jit(solution)/shard_map/all_to_all | solution.py:177
  48.5 0.2 reshape.214
  48.7 1.1 convolution_convert_fusion.4
  49.8 4.6 %all-to-all-start.3 = ((bf16[64,16,256]{2,1,0:T(8,128)(2,1)}), bf16[64,16,256]{2,1,0:T(8,128)(2,1)S(1)}, u32[]{:S(2)}, u32[]{:S(2)}) async-start(bf16[64,16,256]{2,1,0:T(8,128)(2,1)} %bitcast.26), calls=%async_computation.3 | async-start | bytes 1048576 | tf_op jit(solution)/shard_map/all_to_all | solution.py:28
  54.4 0.1 copy.70
  54.5 0.1 eq.29
  54.6 0.2 fusion.11
  54.8 0.1 convert_element_type.98
  54.8 0.1 copy.71
  54.9 0.1 fusion.45
  55.0 0.4 convolution_convert_fusion.1
  55.5 1.3 all_to_all.33
  56.8 15.3 %all-to-all-done.3 = bf16[64,16,256]{2,1,0:T(8,128)(2,1)S(1)} async-done(((bf16[64,16,256]{2,1,0:T(8,128)(2,1)}), bf16[64,16,256]{2,1,0:T(8,128)(2,1)S(1)}, u32[]{:S(2)}, u32[]{:S(2)}) %all-to-all-start.3) | async-done | bytes 524320 | tf_op jit(solution)/shard_map/all_to_all | solution.py:28
  72.0 5.8 %all-to-all-start.1 = ((bf16[64,3,2048]{2,1,0:T(4,128)(2,1)}), bf16[64,3,2048]{2,1,0:T(4,128)(2,1)S(1)}, u32[]{:S(2)}, u32[]{:S(2)}) async-start(bf16[64,3,2048]{2,1,0:T(4,128)(2,1)} %all_to_all.33), calls=%async_computation.1 | async-start | bytes 2097152 | tf_op jit(solution)/shard_map/all_to_all | solution.py:163
  77.8 0.1 convert_reduce_fusion.1
  77.9 0.8 convolution_convert_fusion.2
  78.7 27.9 %all-to-all-done.1 = bf16[64,3,2048]{2,1,0:T(4,128)(2,1)S(1)} async-done(((bf16[64,3,2048]{2,1,0:T(4,128)(2,1)}), bf16[64,3,2048]{2,1,0:T(4,128)(2,1)S(1)}, u32[]{:S(2)}, u32[]{:S(2)}) %all-to-all-start.1) | async-done | bytes 786464 | tf_op jit(solution)/shard_map/all_to_all | solution.py:163
  106.6 2.2 %convolution_bitcast_fusion.1 = f32[64,1,3,256]{3,0,2,1:T(8,128)S(1)} fusion(bf16[1,2048,256]{2,1,0:T(8,128)(2,1)} %param.31, bf16[64,3,2048]{2,1,0:T(4,128)(2,1)S(1)} %all-to-all-done.1), kind=kOutput, calls=%fused_computation.16 | convolution fusion | flops 201326592 | bytes 2031616 | tf_op jit(solution)/shard_map/sjcd,jdf->sjcf/dot_general | solution.py:165
  108.9 2.4 %fusion = bf16[64,1,3,2048]{3,0,2,1:T(8,128)(2,1)S(1)} fusion(bf16[1,256,2048]{2,1,0:T(8,128)(2,1)S(1)} %copy-done, bf16[1,2048,256]{2,1,0:T(8,128)(2,1)} %param.32, bf16[64,3,2048]{2,1,0:T(4,128)(2,1)S(1)} %all-to-all-done.1, f32[64,1,3,256]{3,0,2,1:T(8,128)S(1)} %convolution_bitcast_fusion.1), kind=kOutput, calls=%fused_computation.2 | convolution fusion | flops 403341312 | bytes 3866624 | tf_op jit(solution)/shard_map/sjcf,jfd->sjcd/dot_general | solution.py:172
  111.3 0.7 copy.74
  112.0 0.7 convert_element_type.106
  112.7 0.9 pad_maximum_fusion
  113.6 0.0 copy-start.3
  113.6 0.0 copy-start.10
  113.6 1.0 copy.91
  114.6 4.9 %all-to-all-start.4 = ((bf16[4,208,512]{2,1,0:T(8,128)(2,1)}), bf16[4,208,512]{2,1,0:T(8,128)(2,1)S(1)}, u32[]{:S(2)}, u32[]{:S(2)}) async-start(bf16[4,208,512]{2,1,0:T(8,128)(2,1)} %bitcast.119), calls=%async_computation.4 | async-start | bytes 1703936 | tf_op jit(solution)/shard_map/all_to_all | solution.py:28
  119.6 0.2 fusion.12
  119.8 0.2 fusion.13
  120.1 10.8 %all-to-all-done.4 = bf16[4,208,512]{2,1,0:T(8,128)(2,1)S(1)} async-done(((bf16[4,208,512]{2,1,0:T(8,128)(2,1)}), bf16[4,208,512]{2,1,0:T(8,128)(2,1)S(1)}, u32[]{:S(2)}, u32[]{:S(2)}) %all-to-all-start.4) | async-done | bytes 852000 | tf_op jit(solution)/shard_map/all_to_all | solution.py:28
  130.9 0.1 convert_reduce_fusion
  131.0 0.8 reshape.203
  131.8 5.8 %all-to-all-start.5 = ((bf16[64,3,512]{2,1,0:T(4,128)(2,1)}), bf16[64,3,512]{2,1,0:T(4,128)(2,1)S(1)}, u32[]{:S(2)}, u32[]{:S(2)}) async-start(bf16[64,3,512]{2,1,0:T(4,128)(2,1)} %reshape.203), calls=%async_computation.5 | async-start | bytes 524288 | tf_op jit(solution)/shard_map/all_to_all | solution.py:196
  137.8 0.7 reshape.205
  138.4 0.1 select_reduce_fusion
  138.5 0.1 fusion.17
  138.7 11.9 %all-to-all-done.5 = bf16[64,3,512]{2,1,0:T(4,128)(2,1)S(1)} async-done(((bf16[64,3,512]{2,1,0:T(4,128)(2,1)}), bf16[64,3,512]{2,1,0:T(4,128)(2,1)S(1)}, u32[]{:S(2)}, u32[]{:S(2)}) %all-to-all-start.5) | async-done | bytes 196640 | tf_op jit(solution)/shard_map/all_to_all | solution.py:196
  150.6 0.2 reshape.204
  150.7 0.8 fusion.9
  (39 shorter events, 0.2 us)
Async XLA Ops:
  0.6 108.2 %copy-start = (bf16[1,256,2048]{2,1,0:T(8,128)(2,1)S(1)}, bf16[1,256,2048]{2,1,0:T(8,128)(2,1)}, u32[]{:S(2)}) copy-start(bf16[1,256,2048]{2,1,0:T(8,128)(2,1)} %param.33) | copy-start | bytes 3145732
  3.4 6.4 %copy-start.14 = (s32[16]{0:T(128)S(1)}, s32[16]{0:T(128)}, u32[]{:S(2)}) copy-start(s32[16]{0:T(128)} %param.20) | copy-start | bytes 196
  3.4 6.5 %copy-start.17 = (f32[4]{0:T(128)S(1)}, f32[4]{0:T(128)}, u32[]{:S(2)}) copy-start(f32[4]{0:T(128)} %param.26) | copy-start | bytes 52
  13.1 2.5 %copy-start.1 = (bf16[256,2048]{1,0:T(8,128)(2,1)S(1)}, bf16[256,2048]{1,0:T(8,128)(2,1)}, u32[]{:S(2)}) copy-start(bf16[256,2048]{1,0:T(8,128)(2,1)} %param.27) | copy-start | bytes 3145732
  15.4 10.3 %copy-start.2 = (bf16[16,2048]{1,0:T(8,128)(2,1)S(1)}, bf16[16,2048]{1,0:T(8,128)(2,1)}, u32[]{:S(2)}) copy-start(bf16[16,2048]{1,0:T(8,128)(2,1)} %param.19) | copy-start | bytes 196612
  15.4 10.5 %copy-start.11 = (f32[2048]{0:T(1024)S(1)}, f32[2048]{0:T(1024)}, u32[]{:S(2)}) copy-start(f32[2048]{0:T(1024)} %param.28) | copy-start | bytes 24580
  15.5 33.1 %copy-start.8 = (bf16[32,128]{1,0:T(8,128)(2,1)S(1)}, bf16[32,128]{1,0:T(8,128)(2,1)}, u32[]{:S(2)}) copy-start(bf16[32,128]{1,0:T(8,128)(2,1)} %param.35) | copy-start | bytes 24580
  15.5 33.1 %copy-start.9 = (bf16[32,128]{1,0:T(8,128)(2,1)S(1)}, bf16[32,128]{1,0:T(8,128)(2,1)}, u32[]{:S(2)}) copy-start(bf16[32,128]{1,0:T(8,128)(2,1)} %param.34) | copy-start | bytes 24580
  25.7 28.7 %copy-start.7 = (s32[16,6]{0,1:T(8,128)S(1)}, s32[16,6]{0,1:T(8,128)}, u32[]{:S(2)}) copy-start(s32[16,6]{0,1:T(8,128)} %param.29) | copy-start | bytes 1156
  26.0 29.5 %copy-start.4 = (bf16[16,2048]{1,0:T(8,128)(2,1)}, bf16[16,2048]{1,0:T(8,128)(2,1)S(1)}, u32[]{:S(2)}) copy-start(bf16[16,2048]{1,0:T(8,128)(2,1)S(1)} %multiply_convert_fusion) | copy-start | bytes 196612
  49.8 22.3 %all-to-all-start.3 = ((bf16[64,16,256]{2,1,0:T(8,128)(2,1)}), bf16[64,16,256]{2,1,0:T(8,128)(2,1)S(1)}, u32[]{:S(2)}, u32[]{:S(2)}) async-start(bf16[64,16,256]{2,1,0:T(8,128)(2,1)} %bitcast.26), calls=%async_computation.3 | async-start | bytes 1048576 | tf_op jit(solution)/shard_map/all_to_all | solution.py:28
  55.5 22.4 %copy-start.6 = (bf16[128,2048]{1,0:T(8,128)(2,1)S(1)}, bf16[128,2048]{1,0:T(8,128)(2,1)}, u32[]{:S(2)}) copy-start(bf16[128,2048]{1,0:T(8,128)(2,1)} %param.36) | copy-start | bytes 1572868
  72.0 34.6 %all-to-all-start.1 = ((bf16[64,3,2048]{2,1,0:T(4,128)(2,1)}), bf16[64,3,2048]{2,1,0:T(4,128)(2,1)S(1)}, u32[]{:S(2)}, u32[]{:S(2)}) async-start(bf16[64,3,2048]{2,1,0:T(4,128)(2,1)} %all_to_all.33), calls=%async_computation.1 | async-start | bytes 2097152 | tf_op jit(solution)/shard_map/all_to_all | solution.py:163
  113.6 6.0 %copy-start.3 = (bf16[16,2048]{1,0:T(8,128)(2,1)S(1)}, bf16[16,2048]{1,0:T(8,128)(2,1)}, u32[]{:S(2)}) copy-start(bf16[16,2048]{1,0:T(8,128)(2,1)} %param.19) | copy-start | bytes 196612
  113.6 6.0 %copy-start.10 = (f32[2048]{0:T(1024)S(1)}, f32[2048]{0:T(1024)}, u32[]{:S(2)}) copy-start(f32[2048]{0:T(1024)} %param.22) | copy-start | bytes 24580
  113.6 6.0 %copy-start.15 = (bf16[2048,64]{0,1:T(8,128)(2,1)S(1)}, bf16[2048,64]{0,1:T(8,128)(2,1)}, u32[]{:S(2)}) copy-start(bf16[2048,64]{0,1:T(8,128)(2,1)} %param.24) | copy-start | bytes 786436
  113.6 6.2 %copy-start.16 = (bf16[2048,64]{0,1:T(8,128)(2,1)S(1)}, bf16[2048,64]{0,1:T(8,128)(2,1)}, u32[]{:S(2)}) copy-start(bf16[2048,64]{0,1:T(8,128)(2,1)} %param.25) | copy-start | bytes 786436
  114.6 16.3 %all-to-all-start.4 = ((bf16[4,208,512]{2,1,0:T(8,128)(2,1)}), bf16[4,208,512]{2,1,0:T(8,128)(2,1)S(1)}, u32[]{:S(2)}, u32[]{:S(2)}) async-start(bf16[4,208,512]{2,1,0:T(8,128)(2,1)} %bitcast.119), calls=%async_computation.4 | async-start | bytes 1703936 | tf_op jit(solution)/shard_map/all_to_all | solution.py:28
  119.6 18.1 %copy-start.12 = (bf16[2048]{0:T(1024)(128)(2,1)S(1)}, bf16[2048]{0:T(1024)(128)(2,1)}, u32[]{:S(2)}) copy-start(bf16[2048]{0:T(1024)(128)(2,1)} %param.37) | copy-start | bytes 12292
  119.6 18.9 %copy-start.13 = (f32[16,6]{0,1:T(8,128)S(1)}, f32[16,6]{0,1:T(8,128)}, u32[]{:S(2)}) copy-start(f32[16,6]{0,1:T(8,128)} %param.30) | copy-start | bytes 1156
  119.6 18.9 %copy-start.5 = (bf16[16,2048]{1,0:T(8,128)(2,1)S(1)}, bf16[16,2048]{1,0:T(8,128)(2,1)}, u32[]{:S(2)}) copy-start(bf16[16,2048]{1,0:T(8,128)(2,1)} %copy-done.4) | copy-start | bytes 196612
  131.8 18.7 %all-to-all-start.5 = ((bf16[64,3,512]{2,1,0:T(4,128)(2,1)}), bf16[64,3,512]{2,1,0:T(4,128)(2,1)S(1)}, u32[]{:S(2)}, u32[]{:S(2)}) async-start(bf16[64,3,512]{2,1,0:T(4,128)(2,1)} %reshape.203), calls=%async_computation.5 | async-start | bytes 524288 | tf_op jit(solution)/shard_map/all_to_all | solution.py:196
where the time goes:
time: 155 us; the launch traced here: 152 us
  waiting for transfers between devices  65.9 us (43%)
  blocking collectives  31.8 us (21%)
  starting transfers between devices  21.2 us (14%)
  matrix products  15.4 us (10%)
  local copies, waits for them, and re-layouts  13.4 us (9%)
  other arithmetic  2.89 us (2%)
    all_to_all x1, waiting for transfers between devices, shards(): lax.all_to_all(sent_rows, 'ep', split_axis=0, concat_axis=0, tiled=True)  27.9 us
    all_to_all x2, waiting for transfers between devices, sent_and_summed(): lax.all_to_all(parts, axis, split_axis=0, concat_axis=0, tiled=True)  26.1 us
    all_to_all x1, blocking collectives, shards(): lax.all_to_all(normed_mix, 'ep', split_axis=1, concat_axis=0, tiled=True)  21.9 us
    all_to_all x1, waiting for transfers between devices, shards(): lax.all_to_all(expert_out, 'ep', split_axis=0, concat_axis=0, tiled=True)  11.9 us
    all_to_all x1, blocking collectives, copy_for_each(): return lax.all_to_all(copies, axis, split_axis=0, concat_axis=0, tiled=True)  9.85 us
    all_to_all x2, starting transfers between devices, sent_and_summed(): lax.all_to_all(parts, axis, split_axis=0, concat_axis=0, tiled=True)  9.57 us
    unnamed x41, local copies, waits for them, and re-layouts  6.95 us
    all_to_all x1, starting transfers between devices, shards(): lax.all_to_all(expert_out, 'ep', split_axis=0, concat_axis=0, tiled=True)  5.84 us
  transfers between devices with their start and end apart: 4, of which 4 were waited for; matrix products, arithmetic and copies ran while one was open for 2% of the time, Pallas kernels for 0%

commit v1 on v0

v1 whole, which is shorter than its diff:
```python
import functools

import jax
import jax.numpy as jnp
from jax import lax
from jax.experimental import pallas as pl
from jax.experimental.pallas import tpu as pltpu
from jax.sharding import PartitionSpec as P

HEAD_DIM = 64
EPS = 1e-06
CAP = 3
NY = 4
F32 = jnp.float32
BF16 = jnp.bfloat16
MESH = pl.DeviceIdType.MESH
NT = (((1,), (1,)), ((), ()))


def mm(a, b):
    return jnp.dot(a, b, preferred_element_type=F32)


def silu(v):
    return v / (1.0 + jnp.exp(-v))


def kernel(
    dims,
    tokens,
    lengths,
    cache,
    attn_gain,
    query_weight,
    key_weight,
    value_weight,
    stick_bias,
    out_weight,
    ffn_gain,
    routes,
    route_weights,
    expert_gate,
    expert_up,
    expert_down,
    shared_gate,
    shared_up,
    shared_down,
    gate_vector,
    layer_out,
    new_kv,
    tok_v,
    tokq_v,
    again_v,
    fgain_v,
    gv_v,
    routes_v,
    rw_v,
    wq_v,
    wk_v,
    wv_v,
    wo_v,
    eg_v,
    eu_v,
    ed_v,
    sd_v,
    cache_v,
    sgu_v,
    qrow,
    lrow,
    score,
    orow,
    info,
    take,
    comb,
    att,
    att_in,
    res_v,
    res16,
    tb,
    slot_out,
    xs,
    ys,
    ys_in,
    yy,
    ret,
    zs,
    zs_in,
    sh_out,
    sh_in,
    lsem,
    csem,
    info_s,
    info_r,
    sz_s,
    sz_r,
    sy_s,
    sy_r,
    sc_s,
    sc_r,
    at_s,
    at_r,
    rx_s,
    rx_r,
    tz_s,
    tz_r,
    sl_s,
    sl_r,
    xf_s,
    xf_r,
    yx_s,
    yx_r,
    yg_s,
    yg_r,
    sh_s,
    sh_r,
    zb_s,
    zb_r,
):
    nz, ny, nx = dims
    rows, width = tok_v.shape
    quarter = width // nx
    groups = 2 * ny
    part = CAP * nz
    slots = groups * part
    heads = wq_v.shape[1] // HEAD_DIM
    length = cache_v.shape[1]
    ep = lax.axis_index("ep")
    x = lax.axis_index("tp")
    c = ep % 2
    y = (ep // 2) % ny
    z = ep // (2 * ny)

    def device(z_, y_, c_, x_):
        return ((z_ * ny + y_) * 2 + c_, x_)

    def z_peer(d):
        return device((z + d) % nz, y, c, x)

    def g_peer(g):
        return device(z, (y + g // 2) % ny, (c + g % 2) % 2, x)

    def g_back(g):
        return ((ny - g // 2) % ny) * 2 + g % 2

    def x_peer(d):
        return device(z, y, c, (x + d) % nx)

    def remote(src, dst, send, recv, to):
        copy = pltpu.make_async_remote_copy(
            src_ref=src,
            dst_ref=dst,
            send_sem=send,
            recv_sem=recv,
            device_id=to,
            device_id_type=MESH,
        )
        return copy

    peers = (
        [z_peer(d) for d in range(1, nz)]
        + [g_peer(g) for g in range(1, groups)]
        + [x_peer(d) for d in range(1, nx)]
    )
    barrier = pltpu.get_barrier_semaphore()
    for peer in peers:
        pl.semaphore_signal(barrier, inc=1, device_id=peer, device_id_type=MESH)

    local = {}

    def fetch(name, src, dst):
        copy = pltpu.make_async_copy(src, dst, lsem.at[len(local)])
        copy.start()
        local[name] = copy

    own_q = pl.multiple_of(x * quarter, quarter)
    fetch("tok", tokens, tok_v)
    fetch("again", attn_gain, again_v)
    fetch("wq", query_weight, wq_v)
    fetch("wk", key_weight, wk_v)
    fetch("wv", value_weight, wv_v)
    fetch("routes", routes, routes_v)
    fetch("rw", route_weights, rw_v)
    fetch("sg", shared_gate, sgu_v.at[0, z, y, c])
    fetch("su", shared_up, sgu_v.at[1, z, y, c])
    cached = []
    for n in range(rows):
        copy = pltpu.make_async_copy(cache.at[n], cache_v.at[n], csem.at[n])
        copy.start()
        cached.append(copy)
    fetch("wo", out_weight, wo_v)
    fetch("tokq", tokens.at[:, pl.ds(own_q, quarter)], tokq_v)
    fetch("fgain", ffn_gain, fgain_v)
    fetch("gv", gate_vector, gv_v)
    fetch("eg", expert_gate.at[0], eg_v)
    fetch("eu", expert_up.at[0], eu_v)
    fetch("sd", shared_down, sd_v)
    fetch("ed", expert_down.at[0], ed_v)

    local["tok"].wait()
    local["again"].wait()
    tf = tok_v[...].astype(F32)
    normed = (
        tf * lax.rsqrt(jnp.mean(tf * tf, axis=-1, keepdims=True) + EPS) * again_v[...]
    ).astype(BF16)
    local["wq"].wait()
    q = mm(normed, wq_v[...]).astype(BF16).astype(F32)
    local["wk"].wait()
    local["wv"].wait()
    new_kv[...] = jnp.concatenate(
        [mm(normed, wk_v[...]), mm(normed, wv_v[...])], axis=1
    ).astype(BF16)
    for h in range(heads):
        qrow[pl.ds(h, rows, stride=heads), :] = jnp.concatenate(
            [q[:, h * HEAD_DIM : (h + 1) * HEAD_DIM], jnp.zeros((rows, HEAD_DIM), F32)], axis=1
        )
    local["routes"].wait()
    local["rw"].wait()
    top = routes_v.shape[1]
    info[0] = jnp.concatenate(
        [
            routes_v[...].astype(F32),
            rw_v[...],
            jnp.zeros((rows, info.shape[2] - 2 * top), F32),
        ],
        axis=1,
    )

    pl.semaphore_wait(barrier, len(peers))
    local["sg"].wait()
    local["su"].wait()
    sends = []

    def send(*args):
        copy = remote(*args)
        copy.start()
        sends.append(copy)
        return copy

    info_c, sz_c = [], []
    for d in range(1, nz):
        info_c.append(send(info.at[0], info.at[nz - d], info_s.at[d - 1], info_r.at[d - 1], z_peer(d)))
        own = sgu_v.at[:, z, y, c]
        sz_c.append(send(own, own, sz_s.at[d - 1], sz_r.at[d - 1], z_peer(d)))

    for n in range(rows):
        cached[n].wait()
        at = slice(n * heads, (n + 1) * heads)
        score[at, :] = lax.dot_general(
            qrow[at, :].astype(BF16), cache_v[n], NT, preferred_element_type=F32
        )
        lrow[at, :] = jnp.full((heads, 128), lengths[n], jnp.int32)

    block = 256
    table_r = lax.broadcasted_iota(jnp.int32, (block, block), 0)
    table_c = lax.broadcasted_iota(jnp.int32, (block, block), 1)
    later = jnp.where(table_r > table_c, 1.0, 0.0).astype(BF16)
    all_rows = rows * heads
    head_of = lax.broadcasted_iota(jnp.int32, (all_rows, block), 0) & (heads - 1)
    offset = jnp.zeros((all_rows, block), F32)
    for h in range(heads):
        offset = jnp.where(head_of == h, stick_bias[h], offset)
    limit = jnp.concatenate([lrow[...]] * (block // 128), axis=1)
    beyond = jnp.zeros((all_rows, 1), F32)
    for b in reversed(range(length // block)):
        at = slice(b * block, (b + 1) * block)
        zv = score[:, at] * HEAD_DIM ** (-0.5) + offset
        soft = jnp.log1p(jnp.exp(-jnp.abs(zv)))
        usable = (lax.broadcasted_iota(jnp.int32, (all_rows, block), 1) + b * block) < limit
        keep = jnp.where(usable, jnp.minimum(-zv, 0.0) - soft, 0.0)
        high = keep.astype(BF16)
        low = (keep - high.astype(F32)).astype(BF16)
        within = mm(high, later) + mm(low, later)
        score[:, at] = jnp.where(
            usable, jnp.exp(jnp.minimum(zv, 0.0) - soft + within + beyond), 0.0
        )
        beyond = beyond + within[:, 0:1] + keep[:, 0:1]

    for n in range(rows):
        at = slice(n * heads, (n + 1) * heads)
        orow[at, :] = mm(score[at, :].astype(BF16), cache_v[n])
    heads_out = jnp.concatenate(
        [orow[pl.ds(h, rows, stride=heads), :][:, HEAD_DIM : 2 * HEAD_DIM] for h in range(heads)],
        axis=1,
    ).astype(BF16)
    local["wo"].wait()
    for i in range(nx):
        at = slice(i * quarter, (i + 1) * quarter)
        att[i] = mm(heads_out, wo_v[:, at]).astype(BF16)

    at_c = []
    for d in range(1, nx):
        at_c.append(
            send(att.at[(x + d) % nx], att_in.at[d - 1], at_s.at[d - 1], at_r.at[d - 1], x_peer(d))
        )

    for copy in info_c:
        copy.wait_recv()
    many = nz * rows
    lanes = take.shape[0]
    facts = info[...].reshape(many, info.shape[2])
    lane = lax.broadcasted_iota(jnp.int32, (many, lanes), 1).astype(F32)
    tok_id = lax.broadcasted_iota(jnp.int32, (many, lanes), 0).astype(F32)
    l_group = jnp.floor((lane + 0.5) * (1.0 / part))
    in_group = lane - l_group * part
    l_block = jnp.floor((in_group + 0.5) * (1.0 / CAP))
    l_rank = in_group - l_block * CAP
    l_dy = jnp.floor((l_group + 0.25) * 0.5)
    l_y = y.astype(F32) + l_dy
    l_y = jnp.where(l_y >= ny, l_y - ny, l_y)
    l_c = c.astype(F32) + (l_group - 2.0 * l_dy)
    l_c = jnp.where(l_c >= 2.0, l_c - 2.0, l_c)
    l_expert = (z.astype(F32) * ny + l_y) * 2.0 + l_c
    l_expert = jnp.where(lane < slots, l_expert, -1.0)
    hits = jnp.zeros((many, lanes), F32)
    weigh = jnp.zeros((many, lanes), F32)
    for r in range(top):
        same = facts[:, r : r + 1] == l_expert
        hits = jnp.where(same, 1.0, hits)
        weigh = jnp.where(same, facts[:, top + r : top + r + 1], weigh)
    t_block = jnp.floor((tok_id + 0.5) * (1.0 / rows))
    row_t = lax.broadcasted_iota(jnp.int32, (many, many), 0).astype(F32)
    col_t = lax.broadcasted_iota(jnp.int32, (many, many), 1).astype(F32)
    before = jnp.where(
        (jnp.floor((row_t + 0.5) * (1.0 / rows)) == jnp.floor((col_t + 0.5) * (1.0 / rows)))
        & (col_t < row_t),
        1.0,
        0.0,
    ).astype(BF16)
    rank = mm(before, hits.astype(BF16))
    chosen = (hits > 0.5) & (rank == l_rank) & (t_block == l_block)
    take[...] = jnp.where(chosen, 1.0, 0.0).T.astype(BF16)
    weigh = jnp.where(chosen, weigh, 0.0)
    high = weigh.astype(BF16)
    comb[0] = high
    comb[1] = (weigh - high.astype(F32)).astype(BF16)

    for copy in sz_c:
        copy.wait_recv()
    sy_c = []
    for d in range(1, ny):
        col = sgu_v.at[:, :, y, c]
        sy_c.append(send(col, col, sy_s.at[d - 1], sy_r.at[d - 1], g_peer(2 * d)))

    local["tokq"].wait()
    total = tokq_v[...].astype(F32) + att[x].astype(F32)
    for d in range(1, nx):
        at_c[d - 1].wait_recv()
        total = total + att_in[d - 1].astype(F32)
    res_v[...] = total
    rq = total.astype(BF16)
    tb[0] = rq
    res16[x] = rq
    tz_c = []
    for d in range(1, nz):
        tz_c.append(send(tb.at[0], tb.at[nz - d], tz_s.at[d - 1], tz_r.at[d - 1], z_peer(d)))
    rx_c = []
    for d in range(1, nx):
        rx_c.append(send(res16.at[x], res16.at[x], rx_s.at[d - 1], rx_r.at[d - 1], x_peer(d)))

    for copy in tz_c:
        copy.wait_recv()
    picked = mm(take[0:slots, :], tb[...].reshape(many, quarter))
    xs[x, 0] = picked[0:part].astype(BF16)
    sl_c = {}
    for g in range(1, groups):
        slot_out[g - 1] = picked[g * part : (g + 1) * part].astype(BF16)
        sl_c[g_back(g)] = send(
            slot_out.at[g - 1], xs.at[x, g_back(g)], sl_s.at[g - 1], sl_r.at[g - 1], g_peer(g)
        )
    order = [0, 1] + [s for d in range(1, ny) if d != ny // 2 for s in (2 * d, 2 * d + 1)]
    order += [s for s in range(groups) if s not in order]
    xf_c = {}
    for s in order:
        if s:
            sl_c[s].wait_recv()
        for d in range(1, nx):
            xf_c[s, d] = send(
                xs.at[x, s], xs.at[x, s], xf_s.at[s, d - 1], xf_r.at[s, d - 1], x_peer(d)
            )

    for copy in sy_c:
        copy.wait_recv()
    half = sgu_v.at[:, :, :, c]
    sc_c = send(half, half, sc_s.at[0], sc_r.at[0], g_peer(1))

    local["fgain"].wait()
    local["gv"].wait()
    gain = [fgain_v[:, i * quarter : (i + 1) * quarter] for i in range(nx)]
    for copy in rx_c:
        copy.wait_recv()
    mine = [res16[i].astype(F32) for i in range(nx)]
    square = sum(jnp.sum(m * m, axis=-1, keepdims=True) for m in mine)
    scale = lax.rsqrt(square * (1.0 / width) + EPS)
    mix = [(mine[i] * scale * gain[i]).astype(BF16) for i in range(nx)]
    mix_gate = sum(
        jnp.sum(
            mix[i].astype(F32) * gv_v[:, i * quarter : (i + 1) * quarter].astype(F32),
            axis=-1,
            keepdims=True,
        )
        for i in range(nx)
    )
    mix_gate = 1.0 / (1.0 + jnp.exp(-mix_gate))
    sc_c.wait_recv()
    local["sd"].wait()
    joined = jnp.concatenate(mix, axis=1)
    s_width = sgu_v.shape[-1]
    s_gate = mm(joined, sgu_v[0].reshape(width, s_width))
    s_up = mm(joined, sgu_v[1].reshape(width, s_width))
    s_hidden = (silu(s_gate) * s_up).astype(BF16)
    for i in range(nx):
        sh_out[i] = mm(s_hidden, sd_v[:, i * quarter : (i + 1) * quarter]).astype(BF16)
    sh_c = []
    for d in range(1, nx):
        sh_c.append(
            send(sh_out.at[(x + d) % nx], sh_in.at[d - 1], sh_s.at[d - 1], sh_r.at[d - 1], x_peer(d))
        )

    local["eg"].wait()
    local["eu"].wait()
    local["ed"].wait()
    yx_c = {}
    per = groups // 2
    for half_at in range(2):
        some = order[half_at * per : (half_at + 1) * per]
        for s in some:
            for d in range(1, nx):
                xf_c[s, d].wait_recv()
        pieces = [
            jnp.concatenate([xs[i, s].astype(F32) for s in some], axis=0) for i in range(nx)
        ]
        square = sum(jnp.sum(m * m, axis=-1, keepdims=True) for m in pieces)
        scale = lax.rsqrt(square * (1.0 / width) + EPS)
        feats = jnp.concatenate(
            [(pieces[i] * scale * gain[i]).astype(BF16) for i in range(nx)], axis=1
        )
        hidden = (silu(mm(feats, eg_v[...])) * mm(feats, eu_v[...])).astype(BF16)
        for i in range(nx):
            term = mm(hidden, ed_v[:, i * quarter : (i + 1) * quarter])
            for j, s in enumerate(some):
                ys[i, s] = term[j * part : (j + 1) * part].astype(BF16)
        for s in reversed(some):
            for d in range(1, nx):
                yx_c[s, d] = send(
                    ys.at[(x + d) % nx, s],
                    ys_in.at[d - 1, s],
                    yx_s.at[s, d - 1],
                    yx_r.at[s, d - 1],
                    x_peer(d),
                )

    back = [s for h in range(2) for s in reversed(order[h * per : (h + 1) * per])]
    yg_c = {}
    for s in back:
        total = ys[x, s].astype(F32)
        for d in range(1, nx):
            yx_c[s, d].wait_recv()
            total = total + ys_in[d - 1, s].astype(F32)
        if s == 0:
            ret[0] = total.astype(BF16)
        else:
            yy[s - 1] = total.astype(BF16)
            yg_c[g_back(s)] = send(
                yy.at[s - 1], ret.at[g_back(s)], yg_s.at[s - 1], yg_r.at[s - 1], g_peer(s)
            )
    for s in range(1, groups):
        yg_c[s].wait_recv()
    home = jnp.concatenate([ret[g].astype(F32) for g in range(groups)], axis=0).astype(BF16)
    routed = mm(comb[0][:, 0:slots], home) + mm(comb[1][:, 0:slots], home)
    zb_c = []
    for d in range(1, nz):
        zs[d - 1] = routed[d * rows : (d + 1) * rows].astype(BF16)
        zb_c.append(send(zs.at[d - 1], zs_in.at[d - 1], zb_s.at[d - 1], zb_r.at[d - 1], z_peer(d)))

    shared = sh_out[x].astype(F32)
    for d in range(1, nx):
        sh_c[d - 1].wait_recv()
        shared = shared + sh_in[d - 1].astype(F32)
    final = res_v[...] + mix_gate * shared + routed[0:rows]
    for d in range(1, nz):
        zb_c[d - 1].wait_recv()
        final = final + zs_in[d - 1].astype(F32)
    layer_out[...] = final.astype(BF16)
    for copy in sends:
        copy.wait_send()


def shards(nz, ny, *args):
    (
        tokens,
        lengths,
        cache,
        attn_gain,
        query_weight,
        key_weight,
        value_weight,
        stick_bias,
        out_weight,
        ffn_gain,
        routes,
        route_weights,
        expert_gate,
        expert_up,
        expert_down,
        shared_gate,
        shared_up,
        shared_down,
        gate_vector,
    ) = args
    nx = lax.axis_size("tp")
    rows, width = tokens.shape
    quarter = width // nx
    groups = 2 * ny
    part = CAP * nz
    slots = groups * part
    lanes = -(-slots // 128) * 128
    heads = query_weight.shape[1] // HEAD_DIM
    length = cache.shape[1]
    vm = pltpu.VMEM
    dma = pltpu.SemaphoreType.DMA

    def like(a):
        return vm(a.shape, a.dtype)

    attn_gain = attn_gain.reshape(1, width)
    ffn_gain = ffn_gain.reshape(1, width)
    gate_vector = gate_vector.reshape(1, width)
    scratch = [
        like(tokens),
        vm((rows, quarter), BF16),
        like(attn_gain),
        like(ffn_gain),
        like(gate_vector),
        like(routes),
        like(route_weights),
        like(query_weight),
        like(key_weight),
        like(value_weight),
        like(out_weight),
        vm(expert_gate.shape[1:], BF16),
        vm(expert_up.shape[1:], BF16),
        vm(expert_down.shape[1:], BF16),
        like(shared_down),
        like(cache),
        vm((2, nz, ny, 2, *shared_gate.shape), BF16),
        vm((rows * heads, 2 * HEAD_DIM), F32),
        vm((rows * heads, 128), jnp.int32),
        vm((rows * heads, length), F32),
        vm((rows * heads, 2 * HEAD_DIM), F32),
        vm((nz, rows, 128), F32),
        vm((lanes, nz * rows), BF16),
        vm((2, nz * rows, lanes), BF16),
        vm((nx, rows, quarter), BF16),
        vm((nx - 1, rows, quarter), BF16),
        vm((rows, quarter), F32),
        vm((nx, rows, quarter), BF16),
        vm((nz, rows, quarter), BF16),
        vm((groups - 1, part, quarter), BF16),
        vm((nx, groups, part, quarter), BF16),
        vm((nx, groups, part, quarter), BF16),
        vm((nx - 1, groups, part, quarter), BF16),
        vm((groups - 1, part, quarter), BF16),
        vm((groups, part, quarter), BF16),
        vm((nz - 1, rows, quarter), BF16),
        vm((nz - 1, rows, quarter), BF16),
        vm((nx, rows, quarter), BF16),
        vm((nx - 1, rows, quarter), BF16),
        dma((20,)),
        dma((rows,)),
    ]
    for shape in (
        (nz - 1,),
        (nz - 1,),
        (ny - 1,),
        (1,),
        (nx - 1,),
        (nx - 1,),
        (nz - 1,),
        (groups - 1,),
        (groups, nx - 1),
        (groups, nx - 1),
        (groups - 1,),
        (nx - 1,),
        (nz - 1,),
    ):
        scratch += [dma(shape), dma(shape)]
    spaces = [pl.ANY] * 19
    spaces[1] = pltpu.SMEM
    spaces[7] = pltpu.SMEM
    return pl.pallas_call(
        functools.partial(kernel, (nz, ny, nx)),
        out_shape=(
            jax.ShapeDtypeStruct((rows, quarter), BF16),
            jax.ShapeDtypeStruct((rows, 2 * HEAD_DIM), BF16),
        ),
        in_specs=[pl.BlockSpec(memory_space=s) for s in spaces],
        out_specs=(
            pl.BlockSpec(memory_space=pltpu.VMEM),
            pl.BlockSpec(memory_space=pltpu.VMEM),
        ),
        scratch_shapes=scratch,
        compiler_params=pltpu.CompilerParams(
            collective_id=0, has_side_effects=True, vmem_limit_bytes=48 * 1024 * 1024
        ),
    )(
        tokens,
        lengths,
        cache,
        attn_gain,
        query_weight,
        key_weight,
        value_weight,
        stick_bias,
        out_weight,
        ffn_gain,
        routes,
        route_weights,
        expert_gate,
        expert_up,
        expert_down,
        shared_gate,
        shared_up,
        shared_down,
        gate_vector,
    )


def solution(mesh, ny=NY):
    nz = mesh.shape["ep"] // (2 * ny)
    placed = (
        P("ep", None),
        P("ep"),
        P("ep", None, "tp"),
        P(),
        P(None, "tp"),
        P(None, "tp"),
        P(None, "tp"),
        P("tp"),
        P("tp", None),
        P(),
        P("ep", None),
        P("ep", None),
        P("ep", None, "tp"),
        P("ep", None, "tp"),
        P("ep", "tp", None),
        P("ep", "tp"),
        P("ep", "tp"),
        P("tp", None),
        P(),
    )
    return jax.shard_map(
        functools.partial(shards, nz, ny),
        mesh=mesh,
        in_specs=placed,
        out_specs=(P("ep", "tp"), P("ep", "tp")),
        check_vma=False,
    )
```

time: 155 us -> 73.8 us (0.48); the launches traced: 152 us -> 72.6 us
  waiting for transfers between devices: 65.9 us -> 0 us
  Pallas kernels: 0 us -> 55.2 us
  blocking collectives: 31.8 us -> 0 us
  starting transfers between devices: 21.2 us -> 0 us
  matrix products: 15.4 us -> 0 us
  local copies, waits for them, and re-layouts: 13.4 us -> 16.7 us
  other arithmetic: 2.89 us -> 0 us
    all_to_all x4 -> x0, waiting for transfers between devices: 65.9 us -> none  [the longest x1 27.9 us: shards(): lax.all_to_all(sent_rows, 'ep', split_axis=0, concat_axis=0, tiled=True)]
    pallas_call x0 -> x1, Pallas kernels: none -> 55.2 us  [shards(): pl.pallas_call(functools.partial(kernel, (nz, ny, nx)), out_shape=(jax.Sh...]
    all_to_all x2 -> x0, blocking collectives: 31.8 us -> none  [the longest x1 21.9 us: shards(): lax.all_to_all(normed_mix, 'ep', split_axis=1, concat_axis=0, tiled=True)]
    all_to_all x4 -> x0, starting transfers between devices: 21.2 us -> none  [the longest x2 9.57 us: sent_and_summed(): lax.all_to_all(parts, axis, split_axis=0, concat_axis=0, tiled=True)]
    dot_general x16 -> x0, matrix products: 15.4 us -> none  [the longest x1 2.42 us: shards(): jnp.einsum('sjcf,jfd->sjcd', expert_hidden, expert_down, preferred_elemen...]
    unnamed x41 -> x30, local copies, waits for them, and re-layouts: 6.95 us -> 16 us
    reshape x6 -> x1, local copies, waits for them, and re-layouts: 2.81 us -> 0.69 us  [shards(): gate_vector = gate_vector.reshape(1, width)]
    reduce_sum x7 -> x0, other arithmetic: 1.7 us -> none  [the longest x2 1.2 us: rms_scale(): jnp.mean(values_f * values_f, axis=-1, keepdims=True) + epsilon]
  transfers between devices with their start and end apart: 4 -> 0, of which waited for: 4 -> 0; matrix products, arithmetic and copies ran while one was open for 2% -> 0% of each run, Pallas kernels for 0% -> 0%
where the time goes in v1:
time: 73.8 us; the launch traced here: 72.6 us
  Pallas kernels  55.2 us (75%)
  local copies, waits for them, and re-layouts  16.7 us (23%)
    pallas_call x1, Pallas kernels, shards(): pl.pallas_call(functools.partial(kernel, (nz, ny, nx)), out_shape=(jax.Sh...  55.2 us
    unnamed x30, local copies, waits for them, and re-layouts  16 us

profile of v1, /device:TPU:2, one launch (start us, length us, event | category | flops | bytes accessed | tf_op | source)
XLA Modules:
  0.0 72.6 jit_solution(17253875801125233921)
XLA Ops:
  0.6 0.8 %copy.23.routes = s32[16,6]{1,0:T(8,128)S(1)} copy(s32[16,6]{0,1:T(8,128)} %param.29) | data formatting | bytes 768 | tf_op args[10]
  1.4 0.8 %copy.24.route_weights = f32[16,6]{1,0:T(8,128)S(1)} copy(f32[16,6]{0,1:T(8,128)} %param.30) | data formatting | bytes 768 | tf_op args[11]
  2.2 0.7 reshape.15.gate_vector
  2.9 1.2 %copy.21.key_weight = bf16[2048,64]{1,0:T(8,128)(2,1)S(1)} copy(bf16[2048,64]{0,1:T(8,128)(2,1)} %param.24) | data formatting | bytes 524288 | tf_op args[5]
  4.1 1.2 %copy.22.value_weight = bf16[2048,64]{1,0:T(8,128)(2,1)S(1)} copy(bf16[2048,64]{0,1:T(8,128)(2,1)} %param.25) | data formatting | bytes 524288 | tf_op args[6]
  5.3 0.0 copy-start
  5.3 1.2 %copy-done = bf16[2048,256]{1,0:T(8,128)(2,1)S(1)} copy-done((bf16[2048,256]{1,0:T(8,128)(2,1)S(1)}, bf16[2048,256]{1,0:T(8,128)(2,1)}, u32[]{:S(2)}) %copy-start) | copy-done | bytes 1048600
  6.5 0.0 copy-start.1
  6.5 1.2 %copy-done.1 = bf16[256,2048]{1,0:T(8,128)(2,1)S(1)} copy-done((bf16[256,2048]{1,0:T(8,128)(2,1)S(1)}, bf16[256,2048]{1,0:T(8,128)(2,1)}, u32[]{:S(2)}) %copy-start.1) | copy-done | bytes 1048600
  7.8 0.0 copy-start.2
  7.8 1.2 %copy-done.2 = bf16[1,2048,256]{2,1,0:T(8,128)(2,1)S(1)} copy-done((bf16[1,2048,256]{2,1,0:T(8,128)(2,1)S(1)}, bf16[1,2048,256]{2,1,0:T(8,128)(2,1)}, u32[]{:S(2)}) %copy-start.2) | copy-done | bytes 1048600
  9.0 0.0 copy-start.3
  9.0 1.2 %copy-done.3 = bf16[1,2048,256]{2,1,0:T(8,128)(2,1)S(1)} copy-done((bf16[1,2048,256]{2,1,0:T(8,128)(2,1)S(1)}, bf16[1,2048,256]{2,1,0:T(8,128)(2,1)}, u32[]{:S(2)}) %copy-start.3) | copy-done | bytes 1048600
  10.2 0.0 copy-start.4
  10.2 1.0 %copy-done.4 = bf16[128,2048]{1,0:T(8,128)(2,1)S(1)} copy-done((bf16[128,2048]{1,0:T(8,128)(2,1)S(1)}, bf16[128,2048]{1,0:T(8,128)(2,1)}, u32[]{:S(2)}) %copy-start.4) | copy-done | bytes 524312
  11.3 0.0 copy-start.5
  11.3 0.8 %copy-done.5 = bf16[16,2048]{1,0:T(8,128)(2,1)S(1)} copy-done((bf16[16,2048]{1,0:T(8,128)(2,1)S(1)}, bf16[16,2048]{1,0:T(8,128)(2,1)}, u32[]{:S(2)}) %copy-start.5) | copy-done | bytes 65560
  12.1 0.0 copy-start.6
  12.1 0.7 copy-done.6
  12.8 0.0 copy-start.7
  12.8 0.7 copy-done.7
  13.5 0.0 copy-start.8
  13.5 0.7 copy-done.8
  14.2 0.0 copy-start.9
  14.2 0.7 copy-done.9
  14.9 0.0 copy-start.10
  14.9 0.7 copy-done.10
  15.5 0.0 copy-start.11
  15.5 0.7 copy-done.11
  16.2 55.2 %shard_map.194 = (bf16[16,512]{1,0:T(8,128)(2,1)S(1)}, bf16[16,128]{1,0:T(8,128)(2,1)S(1)}) custom-call(bf16[16,2048]{1,0:T(8,128)(2,1)S(1)} %copy-done.5, s32[16]{0:T(128)S(1)} %copy-done.10, bf16[16,1024,128]{2,1,0:T(8,128)(2,1)} %cache.1, f32[1,2048]{1,0:T(1,128)S(1)} %bitcast.2, bf16[2048,256]{1,0:T(8,128)(2,1)S(1)} %copy-done, ...), custom_call_target="tpu_custom_call" | custom-call | tf_op jit(solution)/shard_map/pallas_call | solution.py:590
  71.4 0.6 copy.27
  72.0 0.6 copy.28
Async XLA Ops:
  5.3 1.2 %copy-start = (bf16[2048,256]{1,0:T(8,128)(2,1)S(1)}, bf16[2048,256]{1,0:T(8,128)(2,1)}, u32[]{:S(2)}) copy-start(bf16[2048,256]{1,0:T(8,128)(2,1)} %query_weight.1) | copy-start | bytes 3145732
  6.5 1.2 %copy-start.1 = (bf16[256,2048]{1,0:T(8,128)(2,1)S(1)}, bf16[256,2048]{1,0:T(8,128)(2,1)}, u32[]{:S(2)}) copy-start(bf16[256,2048]{1,0:T(8,128)(2,1)} %out_weight.1) | copy-start | bytes 3145732
  7.8 1.2 %copy-start.2 = (bf16[1,2048,256]{2,1,0:T(8,128)(2,1)S(1)}, bf16[1,2048,256]{2,1,0:T(8,128)(2,1)}, u32[]{:S(2)}) copy-start(bf16[1,2048,256]{2,1,0:T(8,128)(2,1)} %expert_gate.1) | copy-start | bytes 3145732
  9.0 1.2 %copy-start.3 = (bf16[1,2048,256]{2,1,0:T(8,128)(2,1)S(1)}, bf16[1,2048,256]{2,1,0:T(8,128)(2,1)}, u32[]{:S(2)}) copy-start(bf16[1,2048,256]{2,1,0:T(8,128)(2,1)} %expert_up.1) | copy-start | bytes 3145732
  10.2 1.0 %copy-start.4 = (bf16[128,2048]{1,0:T(8,128)(2,1)S(1)}, bf16[128,2048]{1,0:T(8,128)(2,1)}, u32[]{:S(2)}) copy-start(bf16[128,2048]{1,0:T(8,128)(2,1)} %shared_down.1) | copy-start | bytes 1572868
  11.3 0.8 %copy-start.5 = (bf16[16,2048]{1,0:T(8,128)(2,1)S(1)}, bf16[16,2048]{1,0:T(8,128)(2,1)}, u32[]{:S(2)}) copy-start(bf16[16,2048]{1,0:T(8,128)(2,1)} %tokens.1) | copy-start | bytes 196612
  12.1 0.7 copy-start.6
  12.8 0.7 copy-start.7
  13.5 0.7 copy-start.8
  14.2 0.7 copy-start.9
  14.9 0.7 copy-start.10
  15.5 0.7 copy-start.11

commit v2 on v1

--- a/solution.py
+++ b/solution.py
@@ -19,6 +19,10 @@
 
 def mm(a, b):
     return jnp.dot(a, b, preferred_element_type=F32)
+
+
+def mm_nt(a, b):
+    return lax.dot_general(a, b, NT, preferred_element_type=F32)
 
 
 def silu(v):
@@ -207,7 +211,7 @@
     local["wk"].wait()
     local["wv"].wait()
     new_kv[...] = jnp.concatenate(
-        [mm(normed, wk_v[...]), mm(normed, wv_v[...])], axis=1
+        [mm_nt(normed, wk_v[...]), mm_nt(normed, wv_v[...])], axis=1
     ).astype(BF16)
     for h in range(heads):
         qrow[pl.ds(h, rows, stride=heads), :] = jnp.concatenate(
@@ -215,15 +219,17 @@
         )
     local["routes"].wait()
     local["rw"].wait()
-    top = routes_v.shape[1]
-    info[0] = jnp.concatenate(
+    top = routes_v.shape[0]
+    named = jnp.concatenate(
         [
-            routes_v[...].astype(F32),
-            rw_v[...],
-            jnp.zeros((rows, info.shape[2] - 2 * top), F32),
+            jnp.concatenate([routes_v[...].astype(F32), jnp.zeros((8 - top, rows), F32)], axis=0),
+            jnp.concatenate([rw_v[...], jnp.zeros((8 - top, rows), F32)], axis=0),
         ],
-        axis=1,
+        axis=0,
     )
+    named = jnp.concatenate([named, jnp.zeros((16, 128 - rows), F32)], axis=1)
+    named = jnp.concatenate([named, jnp.zeros((112, 128), F32)], axis=0)
+    info[0] = named.T[0:rows]
 
     pl.semaphore_wait(barrier, len(peers))
     local["sg"].wait()
@@ -245,9 +251,7 @@
     for n in range(rows):
         cached[n].wait()
         at = slice(n * heads, (n + 1) * heads)
-        score[at, :] = lax.dot_general(
-            qrow[at, :].astype(BF16), cache_v[n], NT, preferred_element_type=F32
-        )
+        score[at, :] = mm_nt(qrow[at, :].astype(BF16), cache_v[n])
         lrow[at, :] = jnp.full((heads, 128), lengths[n], jnp.int32)
 
     block = 256
@@ -316,7 +320,7 @@
     for r in range(top):
         same = facts[:, r : r + 1] == l_expert
         hits = jnp.where(same, 1.0, hits)
-        weigh = jnp.where(same, facts[:, top + r : top + r + 1], weigh)
+        weigh = jnp.where(same, facts[:, 8 + r : 9 + r], weigh)
     t_block = jnp.floor((tok_id + 0.5) * (1.0 / rows))
     row_t = lax.broadcasted_iota(jnp.int32, (many, many), 0).astype(F32)
     col_t = lax.broadcasted_iota(jnp.int32, (many, many), 1).astype(F32)
@@ -392,18 +396,15 @@
     square = sum(jnp.sum(m * m, axis=-1, keepdims=True) for m in mine)
     scale = lax.rsqrt(square * (1.0 / width) + EPS)
     mix = [(mine[i] * scale * gain[i]).astype(BF16) for i in range(nx)]
+    joined = jnp.concatenate(mix, axis=1)
+    gv = gv_v[...].astype(F32)
     mix_gate = sum(
-        jnp.sum(
-            mix[i].astype(F32) * gv_v[:, i * quarter : (i + 1) * quarter].astype(F32),
-            axis=-1,
-            keepdims=True,
-        )
-        for i in range(nx)
+        joined[:, i * 128 : (i + 1) * 128].astype(F32) * gv[i : i + 1] for i in range(width // 128)
     )
+    mix_gate = jnp.sum(mix_gate, axis=-1, keepdims=True)
     mix_gate = 1.0 / (1.0 + jnp.exp(-mix_gate))
     sc_c.wait_recv()
     local["sd"].wait()
-    joined = jnp.concatenate(mix, axis=1)
     s_width = sgu_v.shape[-1]
     s_gate = mm(joined, sgu_v[0].reshape(width, s_width))
     s_up = mm(joined, sgu_v[1].reshape(width, s_width))
@@ -522,9 +523,11 @@
     def like(a):
         return vm(a.shape, a.dtype)
 
+    key_weight, value_weight = key_weight.T, value_weight.T
+    routes, route_weights = routes.T, route_weights.T
     attn_gain = attn_gain.reshape(1, width)
     ffn_gain = ffn_gain.reshape(1, width)
-    gate_vector = gate_vector.reshape(1, width)
+    gate_vector = gate_vector.reshape(width // 128, 128)
     scratch = [
         like(tokens),
         vm((rows, quarter), BF16),
@@ -600,7 +603,7 @@
         ),
         scratch_shapes=scratch,
         compiler_params=pltpu.CompilerParams(
-            collective_id=0, has_side_effects=True, vmem_limit_bytes=48 * 1024 * 1024
+            collective_id=0, has_side_effects=True, vmem_limit_bytes=67043328
         ),
     )(
         tokens,

time: 73.8 us -> 60 us (0.81)
  the two profiles are of different devices: /device:TPU:2 before, /device:TPU:8 now
where the time goes in v2:
time: 60 us; the launch traced here: 59.8 us
  Pallas kernels  56.6 us (94%)
  local copies, waits for them, and re-layouts  2.59 us (4%)
  between operations  0.65 us (1%)
    pallas_call x1, Pallas kernels, shards(): pl.pallas_call(functools.partial(kernel, (nz, ny, nx)), out_shape=(jax.Sh...  56.6 us
    unnamed x2, local copies, waits for them, and re-layouts  2.59 us

profile of v2, /device:TPU:8, one launch (start us, length us, event | category | flops | bytes accessed | tf_op | source)
XLA Modules:
  0.0 59.8 jit_solution(12951400800414802390)
XLA Ops:
  0.6 56.6 %shard_map.194 = (bf16[16,512]{1,0:T(8,128)(2,1)}, bf16[16,128]{1,0:T(8,128)(2,1)}) custom-call(bf16[16,2048]{1,0:T(8,128)(2,1)} %tokens.1, s32[16]{0:T(128)} %lengths.1, bf16[16,1024,128]{2,1,0:T(8,128)(2,1)} %cache.1, f32[1,2048]{1,0:T(1,128)} %bitcast.9, bf16[2048,256]{1,0:T(8,128)(2,1)} %query_weight.1, bf16[64,2048]{1,0:T(8,128)(2,1)} %bitcast.7, ...), custom_call_target="tpu_custom_call" | custom-call | tf_op jit(solution)/shard_map/pallas_call | solution.py:593
  57.2 1.3 %copy.23 = bf16[16,512]{1,0:T(8,128)(2,1)} copy(bf16[16,512]{1,0:T(8,128)(2,1)} %get-tuple-element.4) | data formatting | bytes 32768
  58.5 1.3 %copy.24 = bf16[16,128]{1,0:T(8,128)(2,1)} copy(bf16[16,128]{1,0:T(8,128)(2,1)} %get-tuple-element.5) | data formatting | bytes 8192

commit v3 on v2

--- a/solution.py
+++ b/solution.py
@@ -11,6 +11,7 @@
 EPS = 1e-06
 CAP = 3
 NY = 4
+RIGHT = (0, 1, 2, 4, 5)
 F32 = jnp.float32
 BF16 = jnp.bfloat16
 MESH = pl.DeviceIdType.MESH
@@ -52,6 +53,8 @@
     gate_vector,
     layer_out,
     new_kv,
+    len_m,
+    bias_m,
     tok_v,
     tokq_v,
     again_v,
@@ -85,6 +88,8 @@
     xs,
     ys,
     ys_in,
+    opp_in,
+    opp_out,
     yy,
     ret,
     zs,
@@ -93,32 +98,13 @@
     sh_in,
     lsem,
     csem,
-    info_s,
-    info_r,
-    sz_s,
-    sz_r,
-    sy_s,
-    sy_r,
-    sc_s,
-    sc_r,
-    at_s,
-    at_r,
-    rx_s,
-    rx_r,
-    tz_s,
-    tz_r,
-    sl_s,
+    out_s,
+    in_r,
     sl_r,
-    xf_s,
     xf_r,
-    yx_s,
-    yx_r,
-    yg_s,
-    yg_r,
-    sh_s,
-    sh_r,
-    zb_s,
-    zb_r,
+    yo_r,
+    yn_r,
+    xc_r,
 ):
     nz, ny, nx = dims
     rows, width = tok_v.shape
@@ -184,11 +170,15 @@
     fetch("wv", value_weight, wv_v)
     fetch("routes", routes, routes_v)
     fetch("rw", route_weights, rw_v)
+    fetch("len", lengths, len_m)
+    fetch("bias", stick_bias, bias_m)
     fetch("sg", shared_gate, sgu_v.at[0, z, y, c])
     fetch("su", shared_up, sgu_v.at[1, z, y, c])
+    chunk = rows // 4
     cached = []
-    for n in range(rows):
-        copy = pltpu.make_async_copy(cache.at[n], cache_v.at[n], csem.at[n])
+    for n in range(4):
+        at = pl.ds(n * chunk, chunk)
+        copy = pltpu.make_async_copy(cache.at[at], cache_v.at[at], csem.at[n])
         copy.start()
         cached.append(copy)
     fetch("wo", out_weight, wo_v)
@@ -220,39 +210,49 @@
     local["routes"].wait()
     local["rw"].wait()
     top = routes_v.shape[0]
-    named = jnp.concatenate(
+    info[0] = jnp.concatenate(
         [
-            jnp.concatenate([routes_v[...].astype(F32), jnp.zeros((8 - top, rows), F32)], axis=0),
-            jnp.concatenate([rw_v[...], jnp.zeros((8 - top, rows), F32)], axis=0),
+            jnp.concatenate(
+                [routes_v[...].astype(F32), rw_v[...], jnp.zeros((top, 128 - 2 * rows), F32)], axis=1
+            ),
+            jnp.zeros((8 - top, 128), F32),
         ],
         axis=0,
     )
-    named = jnp.concatenate([named, jnp.zeros((16, 128 - rows), F32)], axis=1)
-    named = jnp.concatenate([named, jnp.zeros((112, 128), F32)], axis=0)
-    info[0] = named.T[0:rows]
 
     pl.semaphore_wait(barrier, len(peers))
     local["sg"].wait()
     local["su"].wait()
-    sends = []
-
-    def send(*args):
-        copy = remote(*args)
-        copy.start()
-        sends.append(copy)
-        return copy
-
-    info_c, sz_c = [], []
-    for d in range(1, nz):
-        info_c.append(send(info.at[0], info.at[nz - d], info_s.at[d - 1], info_r.at[d - 1], z_peer(d)))
-        own = sgu_v.at[:, z, y, c]
-        sz_c.append(send(own, own, sz_s.at[d - 1], sz_r.at[d - 1], z_peer(d)))
-
+    INFO, SZ, SY, SC, AT, RX, TZ, SL, XF, YX, YG, SH, ZB = range(13)
+    LAST = SL
+    posted = {}
+
+    def send(step, src, dst, recv, to, total):
+        posted[step] = total
+        remote(src, dst, out_s.at[step], recv, to).start()
+
+    def arrived(ref, sem):
+        pltpu.make_async_copy(ref, ref, sem).wait()
+
+    far_z = sorted(range(1, nz), key=lambda d: -min(d, nz - d))
+    far_y = sorted(range(1, ny), key=lambda d: -min(d, ny - d))
+    far_x = sorted(range(1, nx), key=lambda d: -min(d, nx - d))
+    others = info.at[pl.ds(1, nz - 1)]
+    columns = sgu_v.at[:, pl.ds(0, nz - 1), 0, 0]
+    own = sgu_v.at[:, z, y, c]
+    for d in far_z:
+        send(SZ, own, own, in_r.at[SZ], z_peer(d), columns)
+    for d in far_z:
+        send(INFO, info.at[0], info.at[nz - d], in_r.at[INFO], z_peer(d), others)
+
+    local["len"].wait()
+    local["bias"].wait()
     for n in range(rows):
-        cached[n].wait()
+        if n % chunk == 0:
+            cached[n // chunk].wait()
         at = slice(n * heads, (n + 1) * heads)
         score[at, :] = mm_nt(qrow[at, :].astype(BF16), cache_v[n])
-        lrow[at, :] = jnp.full((heads, 128), lengths[n], jnp.int32)
+        lrow[at, :] = jnp.full((heads, 128), len_m[n], jnp.int32)
 
     block = 256
     table_r = lax.broadcasted_iota(jnp.int32, (block, block), 0)
@@ -262,7 +262,7 @@
     head_of = lax.broadcasted_iota(jnp.int32, (all_rows, block), 0) & (heads - 1)
     offset = jnp.zeros((all_rows, block), F32)
     for h in range(heads):
-        offset = jnp.where(head_of == h, stick_bias[h], offset)
+        offset = jnp.where(head_of == h, bias_m[h], offset)
     limit = jnp.concatenate([lrow[...]] * (block // 128), axis=1)
     beyond = jnp.zeros((all_rows, 1), F32)
     for b in reversed(range(length // block)):
@@ -291,17 +291,31 @@
         at = slice(i * quarter, (i + 1) * quarter)
         att[i] = mm(heads_out, wo_v[:, at]).astype(BF16)
 
-    at_c = []
+    for d in far_x:
+        send(AT, att.at[(x + d) % nx], att_in.at[d - 1], in_r.at[AT], x_peer(d), att_in)
+
+    local["tokq"].wait()
+    total = tokq_v[...].astype(F32) + att[x].astype(F32)
+    arrived(att_in, in_r.at[AT])
     for d in range(1, nx):
-        at_c.append(
-            send(att.at[(x + d) % nx], att_in.at[d - 1], at_s.at[d - 1], at_r.at[d - 1], x_peer(d))
-        )
-
-    for copy in info_c:
-        copy.wait_recv()
+        total = total + att_in[d - 1].astype(F32)
+    res_v[...] = total
+    rq = total.astype(BF16)
+    tb[0] = rq
+    res16[x] = rq
+    blocks = tb.at[pl.ds(1, nz - 1)]
+    for d in far_z:
+        send(TZ, tb.at[0], tb.at[nz - d], in_r.at[TZ], z_peer(d), blocks)
+    for d in far_x:
+        send(RX, res16.at[x], res16.at[x], in_r.at[RX], x_peer(d), att_in)
+
+    arrived(others, in_r.at[INFO])
     many = nz * rows
     lanes = take.shape[0]
-    facts = info[...].reshape(many, info.shape[2])
+    facts = info[...].reshape(nz * 8, 128)
+    facts = jnp.concatenate([facts, jnp.zeros((128 - nz * 8, 128), F32)], axis=0).T
+    names = jnp.concatenate([facts[0:rows, d * 8 : d * 8 + 8] for d in range(nz)], axis=0)
+    shares = jnp.concatenate([facts[rows : 2 * rows, d * 8 : d * 8 + 8] for d in range(nz)], axis=0)
     lane = lax.broadcasted_iota(jnp.int32, (many, lanes), 1).astype(F32)
     tok_id = lax.broadcasted_iota(jnp.int32, (many, lanes), 0).astype(F32)
     l_group = jnp.floor((lane + 0.5) * (1.0 / part))
@@ -318,9 +332,9 @@
     hits = jnp.zeros((many, lanes), F32)
     weigh = jnp.zeros((many, lanes), F32)
     for r in range(top):
-        same = facts[:, r : r + 1] == l_expert
+        same = names[:, r : r + 1] == l_expert
         hits = jnp.where(same, 1.0, hits)
-        weigh = jnp.where(same, facts[:, 8 + r : 9 + r], weigh)
+        weigh = jnp.where(same, shares[:, r : r + 1], weigh)
     t_block = jnp.floor((tok_id + 0.5) * (1.0 / rows))
     row_t = lax.broadcasted_iota(jnp.int32, (many, many), 0).astype(F32)
     col_t = lax.broadcasted_iota(jnp.int32, (many, many), 1).astype(F32)
@@ -338,95 +352,70 @@
     comb[0] = high
     comb[1] = (weigh - high.astype(F32)).astype(BF16)
 
-    for copy in sz_c:
-        copy.wait_recv()
-    sy_c = []
-    for d in range(1, ny):
-        col = sgu_v.at[:, :, y, c]
-        sy_c.append(send(col, col, sy_s.at[d - 1], sy_r.at[d - 1], g_peer(2 * d)))
-
-    local["tokq"].wait()
-    total = tokq_v[...].astype(F32) + att[x].astype(F32)
-    for d in range(1, nx):
-        at_c[d - 1].wait_recv()
-        total = total + att_in[d - 1].astype(F32)
-    res_v[...] = total
-    rq = total.astype(BF16)
-    tb[0] = rq
-    res16[x] = rq
-    tz_c = []
-    for d in range(1, nz):
-        tz_c.append(send(tb.at[0], tb.at[nz - d], tz_s.at[d - 1], tz_r.at[d - 1], z_peer(d)))
-    rx_c = []
-    for d in range(1, nx):
-        rx_c.append(send(res16.at[x], res16.at[x], rx_s.at[d - 1], rx_r.at[d - 1], x_peer(d)))
-
-    for copy in tz_c:
-        copy.wait_recv()
+    arrived(columns, in_r.at[SZ])
+    three = sgu_v.at[:, :, pl.ds(0, 3), 0]
+    near = sgu_v.at[:, :, y, c]
+    for d in (1, ny - 1):
+        send(SY, near, near, in_r.at[SY], g_peer(2 * d), three)
+
+    arrived(blocks, in_r.at[TZ])
     picked = mm(take[0:slots, :], tb[...].reshape(many, quarter))
     xs[x, 0] = picked[0:part].astype(BF16)
-    sl_c = {}
-    for g in range(1, groups):
+    for g in [2 * d + k for d in far_y for k in range(2)] + [1]:
         slot_out[g - 1] = picked[g * part : (g + 1) * part].astype(BF16)
-        sl_c[g_back(g)] = send(
-            slot_out.at[g - 1], xs.at[x, g_back(g)], sl_s.at[g - 1], sl_r.at[g - 1], g_peer(g)
-        )
-    order = [0, 1] + [s for d in range(1, ny) if d != ny // 2 for s in (2 * d, 2 * d + 1)]
-    order += [s for s in range(groups) if s not in order]
-    xf_c = {}
-    for s in order:
-        if s:
-            sl_c[s].wait_recv()
-        for d in range(1, nx):
-            xf_c[s, d] = send(
-                xs.at[x, s], xs.at[x, s], xf_s.at[s, d - 1], xf_r.at[s, d - 1], x_peer(d)
-            )
-
-    for copy in sy_c:
-        copy.wait_recv()
-    half = sgu_v.at[:, :, :, c]
-    sc_c = send(half, half, sc_s.at[0], sc_r.at[0], g_peer(1))
-
-    local["fgain"].wait()
-    local["gv"].wait()
-    gain = [fgain_v[:, i * quarter : (i + 1) * quarter] for i in range(nx)]
-    for copy in rx_c:
-        copy.wait_recv()
-    mine = [res16[i].astype(F32) for i in range(nx)]
-    square = sum(jnp.sum(m * m, axis=-1, keepdims=True) for m in mine)
-    scale = lax.rsqrt(square * (1.0 / width) + EPS)
-    mix = [(mine[i] * scale * gain[i]).astype(BF16) for i in range(nx)]
-    joined = jnp.concatenate(mix, axis=1)
-    gv = gv_v[...].astype(F32)
-    mix_gate = sum(
-        joined[:, i * 128 : (i + 1) * 128].astype(F32) * gv[i : i + 1] for i in range(width // 128)
-    )
-    mix_gate = jnp.sum(mix_gate, axis=-1, keepdims=True)
-    mix_gate = 1.0 / (1.0 + jnp.exp(-mix_gate))
-    sc_c.wait_recv()
-    local["sd"].wait()
-    s_width = sgu_v.shape[-1]
-    s_gate = mm(joined, sgu_v[0].reshape(width, s_width))
-    s_up = mm(joined, sgu_v[1].reshape(width, s_width))
-    s_hidden = (silu(s_gate) * s_up).astype(BF16)
-    for i in range(nx):
-        sh_out[i] = mm(s_hidden, sd_v[:, i * quarter : (i + 1) * quarter]).astype(BF16)
-    sh_c = []
-    for d in range(1, nx):
-        sh_c.append(
-            send(sh_out.at[(x + d) % nx], sh_in.at[d - 1], sh_s.at[d - 1], sh_r.at[d - 1], x_peer(d))
-        )
-
-    local["eg"].wait()
-    local["eu"].wait()
-    local["ed"].wait()
-    yx_c = {}
-    per = groups // 2
-    for half_at in range(2):
-        some = order[half_at * per : (half_at + 1) * per]
-        for s in some:
-            for d in range(1, nx):
-                xf_c[s, d].wait_recv()
+        send(SL, slot_out.at[g - 1], xs.at[x, g_back(g)], sl_r.at[g_back(g)], g_peer(g), slot_out)
+    order = [0, 1] + [2 * d + k for d in reversed(far_y) for k in range(2)]
+    right, left = (x + 1) % nx, (x + nx - 1) % nx
+    pairs = [order[i : i + 2] for i in range(0, groups, 2)]
+    direct = pairs[-1]
+    rightward = [s for at, s in enumerate(order) if at in RIGHT]
+    chunks = xs.at[pl.ds(0, 3)]
+
+    def rest(s):
+        return xc_r.at[order.index(s) // 2]
+
+    def gather_send(s):
+        here = xs.at[x, s]
+        for d in far_x if s in direct else (1, nx - 1):
+            first = s not in direct and (d == 1) == (s in rightward)
+            send(XF, here, here, xf_r.at[s] if first else rest(s), x_peer(d), chunks)
+
+    def gather_pass(s):
+        here = xs.at[left if s in rightward else right, s]
+        arrived(here, xf_r.at[s])
+        send(XF, here, here, rest(s), x_peer(1 if s in rightward else nx - 1), chunks)
+
+    parts = ys.at[pl.ds(0, 3)]
+
+    def sum_send(s):
+        if s in direct:
+            for d in far_x:
+                send(YX, ys.at[(x + d) % nx, s], ys_in.at[s, d - 1], yn_r.at[s], x_peer(d), parts)
+            return
+        on, off = (1, nx - 1) if s in rightward else (nx - 1, 1)
+        send(YX, ys.at[(x + 2) % nx, s], opp_in.at[s], yo_r.at[s], x_peer(on), parts)
+        send(YX, ys.at[(x + off) % nx, s], ys_in.at[s, 0], yn_r.at[s], x_peer(off), parts)
+
+    def sum_pass(s):
+        on = 1 if s in rightward else nx - 1
+        arrived(opp_in.at[s], yo_r.at[s])
+        opp_out[s] = (ys[(x + on) % nx, s].astype(F32) + opp_in[s].astype(F32)).astype(BF16)
+        send(YX, opp_out.at[s], ys_in.at[s, 1], yn_r.at[s], x_peer(on), parts)
+
+    def sum_end(s):
+        count = nx - 1 if s in direct else 2
+        arrived(ys_in.at[s, pl.ds(0, count)], yn_r.at[s])
+        total = ys[x, s].astype(F32)
+        for i in range(count):
+            total = total + ys_in[s, i].astype(F32)
+        if s == 0:
+            ret[0] = total.astype(BF16)
+        else:
+            yy[s - 1] = total.astype(BF16)
+            send(YG, yy.at[s - 1], ret.at[g_back(s)], in_r.at[YG], g_peer(s), yy)
+
+    def experts(some):
+        arrived(xs.at[0, pl.ds(0, 6 if some == direct else 4)], rest(some[0]))
         pieces = [
             jnp.concatenate([xs[i, s].astype(F32) for s in some], axis=0) for i in range(nx)
         ]
@@ -440,50 +429,90 @@
             term = mm(hidden, ed_v[:, i * quarter : (i + 1) * quarter])
             for j, s in enumerate(some):
                 ys[i, s] = term[j * part : (j + 1) * part].astype(BF16)
-        for s in reversed(some):
-            for d in range(1, nx):
-                yx_c[s, d] = send(
-                    ys.at[(x + d) % nx, s],
-                    ys_in.at[d - 1, s],
-                    yx_s.at[s, d - 1],
-                    yx_r.at[s, d - 1],
-                    x_peer(d),
-                )
-
-    back = [s for h in range(2) for s in reversed(order[h * per : (h + 1) * per])]
-    yg_c = {}
-    for s in back:
-        total = ys[x, s].astype(F32)
-        for d in range(1, nx):
-            yx_c[s, d].wait_recv()
-            total = total + ys_in[d - 1, s].astype(F32)
-        if s == 0:
-            ret[0] = total.astype(BF16)
-        else:
-            yy[s - 1] = total.astype(BF16)
-            yg_c[g_back(s)] = send(
-                yy.at[s - 1], ret.at[g_back(s)], yg_s.at[s - 1], yg_r.at[s - 1], g_peer(s)
-            )
-    for s in range(1, groups):
-        yg_c[s].wait_recv()
+        for s in some:
+            sum_send(s)
+
+    local["fgain"].wait()
+    local["gv"].wait()
+    gain = [fgain_v[:, i * quarter : (i + 1) * quarter] for i in range(nx)]
+    for name in ("eg", "eu", "ed"):
+        local[name].wait()
+
+    gather_send(0)
+    arrived(xs.at[x, 1], sl_r.at[1])
+    gather_send(1)
+    gather_pass(0)
+    for at, s in enumerate(order[2:]):
+        arrived(xs.at[x, s], sl_r.at[s])
+        gather_send(s)
+        if at == 1:
+            gather_pass(1)
+    for s in pairs[1]:
+        gather_pass(s)
+    experts(pairs[0])
+    arrived(sgu_v.at[:, :, pl.ds(0, 2), 0], in_r.at[SY])
+    mid = nz // 2
+    low_half = sgu_v.at[:, pl.ds(0, mid), (y + ny - 1) % ny, c]
+    high_half = sgu_v.at[:, pl.ds(mid, mid), (y + 1) % ny, c]
+    send(SY, low_half, low_half, in_r.at[SC], g_peer(2), three)
+    send(SY, high_half, high_half, in_r.at[SC], g_peer(2 * (ny - 1)), three)
+    for s in order[4:-2]:
+        gather_pass(s)
+    experts(pairs[1])
+    for s in pairs[0]:
+        sum_pass(s)
+    for pair in pairs[2:]:
+        experts(pair)
+    for s in order[2:-2]:
+        sum_pass(s)
+
+    arrived(near, in_r.at[SC])
+    half = sgu_v.at[:, :, :, c]
+    send(SC, half, half, in_r.at[SH], g_peer(1), sgu_v.at[:, :, :, 0])
+    for s in order:
+        sum_end(s)
+
+    arrived(att_in, in_r.at[RX])
+    mine = [res16[i].astype(F32) for i in range(nx)]
+    square = sum(jnp.sum(m * m, axis=-1, keepdims=True) for m in mine)
+    scale = lax.rsqrt(square * (1.0 / width) + EPS)
+    mix = [(mine[i] * scale * gain[i]).astype(BF16) for i in range(nx)]
+    joined = jnp.concatenate(mix, axis=1)
+    gv = gv_v[...].astype(F32)
+    mix_gate = sum(
+        joined[:, i * 128 : (i + 1) * 128].astype(F32) * gv[i : i + 1] for i in range(width // 128)
+    )
+    mix_gate = jnp.sum(mix_gate, axis=-1, keepdims=True)
+    mix_gate = 1.0 / (1.0 + jnp.exp(-mix_gate))
+    arrived(half, in_r.at[SH])
+    local["sd"].wait()
+    s_width = sgu_v.shape[-1]
+    s_gate = mm(joined, sgu_v[0].reshape(width, s_width))
+    s_up = mm(joined, sgu_v[1].reshape(width, s_width))
+    s_hidden = (silu(s_gate) * s_up).astype(BF16)
+    for i in range(nx):
+        sh_out[i] = mm(s_hidden, sd_v[:, i * quarter : (i + 1) * quarter]).astype(BF16)
+    for d in far_x:
+        send(SH, sh_out.at[(x + d) % nx], sh_in.at[d - 1], in_r.at[ZB], x_peer(d), sh_in)
+
+    arrived(ret.at[pl.ds(1, groups - 1)], in_r.at[YG])
     home = jnp.concatenate([ret[g].astype(F32) for g in range(groups)], axis=0).astype(BF16)
     routed = mm(comb[0][:, 0:slots], home) + mm(comb[1][:, 0:slots], home)
-    zb_c = []
-    for d in range(1, nz):
+    for d in far_z:
         zs[d - 1] = routed[d * rows : (d + 1) * rows].astype(BF16)
-        zb_c.append(send(zs.at[d - 1], zs_in.at[d - 1], zb_s.at[d - 1], zb_r.at[d - 1], z_peer(d)))
-
+        send(ZB, zs.at[d - 1], zs_in.at[d - 1], in_r.at[LAST], z_peer(d), zs)
+
+    arrived(sh_in, in_r.at[ZB])
     shared = sh_out[x].astype(F32)
     for d in range(1, nx):
-        sh_c[d - 1].wait_recv()
         shared = shared + sh_in[d - 1].astype(F32)
     final = res_v[...] + mix_gate * shared + routed[0:rows]
+    arrived(zs_in, in_r.at[LAST])
     for d in range(1, nz):
-        zb_c[d - 1].wait_recv()
         final = final + zs_in[d - 1].astype(F32)
     layer_out[...] = final.astype(BF16)
-    for copy in sends:
-        copy.wait_send()
+    for step, total in posted.items():
+        arrived(total, out_s.at[step])
 
 
 def shards(nz, ny, *args):
@@ -529,6 +558,8 @@
     ffn_gain = ffn_gain.reshape(1, width)
     gate_vector = gate_vector.reshape(width // 128, 128)
     scratch = [
+        pltpu.SMEM(lengths.shape, lengths.dtype),
+        pltpu.SMEM(stick_bias.shape, stick_bias.dtype),
         like(tokens),
         vm((rows, quarter), BF16),
         like(attn_gain),
@@ -550,7 +581,7 @@
         vm((rows * heads, 128), jnp.int32),
         vm((rows * heads, length), F32),
         vm((rows * heads, 2 * HEAD_DIM), F32),
-        vm((nz, rows, 128), F32),
+        vm((nz, 8, 128), F32),
         vm((lanes, nz * rows), BF16),
         vm((2, nz * rows, lanes), BF16),
         vm((nx, rows, quarter), BF16),
@@ -561,51 +592,21 @@
         vm((groups - 1, part, quarter), BF16),
         vm((nx, groups, part, quarter), BF16),
         vm((nx, groups, part, quarter), BF16),
-        vm((nx - 1, groups, part, quarter), BF16),
+        vm((groups, 3, part, quarter), BF16),
+        vm((groups, part, quarter), BF16),
+        vm((groups, part, quarter), BF16),
         vm((groups - 1, part, quarter), BF16),
         vm((groups, part, quarter), BF16),
         vm((nz - 1, rows, quarter), BF16),
         vm((nz - 1, rows, quarter), BF16),
         vm((nx, rows, quarter), BF16),
         vm((nx - 1, rows, quarter), BF16),
-        dma((20,)),
-        dma((rows,)),
+        dma((24,)),
+        dma((4,)),
     ]
-    for shape in (
-        (nz - 1,),
-        (nz - 1,),
-        (ny - 1,),
-        (1,),
-        (nx - 1,),
-        (nx - 1,),
-        (nz - 1,),
-        (groups - 1,),
-        (groups, nx - 1),
-        (groups, nx - 1),
-        (groups - 1,),
-        (nx - 1,),
-        (nz - 1,),
-    ):
-        scratch += [dma(shape), dma(shape)]
-    spaces = [pl.ANY] * 19
-    spaces[1] = pltpu.SMEM
-    spaces[7] = pltpu.SMEM
-    return pl.pallas_call(
-        functools.partial(kernel, (nz, ny, nx)),
-        out_shape=(
-            jax.ShapeDtypeStruct((rows, quarter), BF16),
-            jax.ShapeDtypeStruct((rows, 2 * HEAD_DIM), BF16),
-        ),
-        in_specs=[pl.BlockSpec(memory_space=s) for s in spaces],
-        out_specs=(
-            pl.BlockSpec(memory_space=pltpu.VMEM),
-            pl.BlockSpec(memory_space=pltpu.VMEM),
-        ),
-        scratch_shapes=scratch,
-        compiler_params=pltpu.CompilerParams(
-            collective_id=0, has_side_effects=True, vmem_limit_bytes=67043328
-        ),
-    )(
+    scratch += [dma((13,)), dma((13,))] + [dma((groups,)) for _ in range(5)]
+    spaces = [pltpu.HBM] * 19
+    operands = (
         tokens,
         lengths,
         cache,
@@ -626,6 +627,22 @@
         shared_down,
         gate_vector,
     )
+    return pl.pallas_call(
+        functools.partial(kernel, (nz, ny, nx)),
+        out_shape=(
+            jax.ShapeDtypeStruct((rows, quarter), BF16),
+            jax.ShapeDtypeStruct((rows, 2 * HEAD_DIM), BF16),
+        ),
+        in_specs=[pl.BlockSpec(memory_space=s) for s in spaces],
+        out_specs=(
+            pl.BlockSpec(memory_space=pltpu.VMEM),
+            pl.BlockSpec(memory_space=pltpu.VMEM),
+        ),
+        scratch_shapes=scratch,
+        compiler_params=pltpu.CompilerParams(
+            collective_id=0, has_side_effects=True, vmem_limit_bytes=48 * 1024 * 1024
+        ),
+    )(*[pltpu.with_memory_space_constraint(a, pltpu.HBM) for a in operands])
 
 
 def solution(mesh, ny=NY):

time: 60 us -> 55.4 us (0.923)
  the two profiles are of different devices: /device:TPU:8 before, /device:TPU:2 now
where the time goes in v3:
time: 55.4 us; the launch traced here: 54.3 us
  Pallas kernels  52.5 us (95%)
  local copies, waits for them, and re-layouts  1.2 us (2%)
  between operations  0.65 us (1%)
    pallas_call x1, Pallas kernels, shards(): pl.pallas_call(functools.partial(kernel, (nz, ny, nx)), out_shape=(jax.Sh...  52.5 us
    unnamed x2, local copies, waits for them, and re-layouts  1.2 us

profile of v3, /device:TPU:2, one launch (start us, length us, event | category | flops | bytes accessed | tf_op | source)
XLA Modules:
  0.0 54.3 jit_solution(7296135477380376135)
XLA Ops:
  0.6 52.5 %shard_map.194 = (bf16[16,512]{1,0:T(8,128)(2,1)S(1)}, bf16[16,128]{1,0:T(8,128)(2,1)S(1)}) custom-call(bf16[16,2048]{1,0:T(8,128)(2,1)} %tokens.1, s32[16]{0:T(128)} %lengths.1, bf16[16,1024,128]{2,1,0:T(8,128)(2,1)} %cache.1, f32[1,2048]{1,0:T(1,128)} %bitcast.9, bf16[2048,256]{1,0:T(8,128)(2,1)} %query_weight.1, bf16[64,2048]{1,0:T(8,128)(2,1)} %bitcast.7, ...), custom_call_target="tpu_custom_call" | custom-call | tf_op jit(solution)/shard_map/pallas_call | solution.py:630
  53.1 0.6 %copy.23 = bf16[16,512]{1,0:T(8,128)(2,1)} copy(bf16[16,512]{1,0:T(8,128)(2,1)S(1)} %get-tuple-element.4) | data formatting | bytes 32768
  53.7 0.6 %copy.24 = bf16[16,128]{1,0:T(8,128)(2,1)} copy(bf16[16,128]{1,0:T(8,128)(2,1)S(1)} %get-tuple-element.5) | data formatting | bytes 8192

commit v4 on v3

--- a/solution.py
+++ b/solution.py
@@ -11,7 +11,9 @@
 EPS = 1e-06
 CAP = 3
 NY = 4
-RIGHT = (0, 1, 2, 4, 5)
+GATHER_RIGHT = (1, 3, 5, 7)
+SUM_RIGHT = (0, 1, 4, 5)
+SUM_DIRECT = 1
 F32 = jnp.float32
 BF16 = jnp.bfloat16
 MESH = pl.DeviceIdType.MESH
@@ -151,10 +153,6 @@
         + [g_peer(g) for g in range(1, groups)]
         + [x_peer(d) for d in range(1, nx)]
     )
-    barrier = pltpu.get_barrier_semaphore()
-    for peer in peers:
-        pl.semaphore_signal(barrier, inc=1, device_id=peer, device_id_type=MESH)
-
     local = {}
 
     def fetch(name, src, dst):
@@ -168,12 +166,16 @@
     fetch("wq", query_weight, wq_v)
     fetch("wk", key_weight, wk_v)
     fetch("wv", value_weight, wv_v)
+    fetch("len", lengths, len_m)
+    fetch("bias", stick_bias, bias_m)
     fetch("routes", routes, routes_v)
     fetch("rw", route_weights, rw_v)
-    fetch("len", lengths, len_m)
-    fetch("bias", stick_bias, bias_m)
-    fetch("sg", shared_gate, sgu_v.at[0, z, y, c])
-    fetch("su", shared_up, sgu_v.at[1, z, y, c])
+    barrier = pltpu.get_barrier_semaphore()
+    for peer in peers:
+        pl.semaphore_signal(barrier, inc=1, device_id=peer, device_id_type=MESH)
+
+    local["tok"].wait()
+    local["again"].wait()
     chunk = rows // 4
     cached = []
     for n in range(4):
@@ -181,17 +183,6 @@
         copy = pltpu.make_async_copy(cache.at[at], cache_v.at[at], csem.at[n])
         copy.start()
         cached.append(copy)
-    fetch("wo", out_weight, wo_v)
-    fetch("tokq", tokens.at[:, pl.ds(own_q, quarter)], tokq_v)
-    fetch("fgain", ffn_gain, fgain_v)
-    fetch("gv", gate_vector, gv_v)
-    fetch("eg", expert_gate.at[0], eg_v)
-    fetch("eu", expert_up.at[0], eu_v)
-    fetch("sd", shared_down, sd_v)
-    fetch("ed", expert_down.at[0], ed_v)
-
-    local["tok"].wait()
-    local["again"].wait()
     tf = tok_v[...].astype(F32)
     normed = (
         tf * lax.rsqrt(jnp.mean(tf * tf, axis=-1, keepdims=True) + EPS) * again_v[...]
@@ -207,6 +198,16 @@
         qrow[pl.ds(h, rows, stride=heads), :] = jnp.concatenate(
             [q[:, h * HEAD_DIM : (h + 1) * HEAD_DIM], jnp.zeros((rows, HEAD_DIM), F32)], axis=1
         )
+    fetch("wo", out_weight, wo_v)
+    fetch("tokq", tokens.at[:, pl.ds(own_q, quarter)], tokq_v)
+    fetch("fgain", ffn_gain, fgain_v)
+    fetch("gv", gate_vector, gv_v)
+    fetch("sg", shared_gate, sgu_v.at[0, z, y, c])
+    fetch("su", shared_up, sgu_v.at[1, z, y, c])
+    fetch("eg", expert_gate.at[0], eg_v)
+    fetch("eu", expert_up.at[0], eu_v)
+    fetch("sd", shared_down, sd_v)
+    fetch("ed", expert_down.at[0], ed_v)
     local["routes"].wait()
     local["rw"].wait()
     top = routes_v.shape[0]
@@ -220,9 +221,6 @@
         axis=0,
     )
 
-    pl.semaphore_wait(barrier, len(peers))
-    local["sg"].wait()
-    local["su"].wait()
     INFO, SZ, SY, SC, AT, RX, TZ, SL, XF, YX, YG, SH, ZB = range(13)
     LAST = SL
     posted = {}
@@ -237,14 +235,6 @@
     far_z = sorted(range(1, nz), key=lambda d: -min(d, nz - d))
     far_y = sorted(range(1, ny), key=lambda d: -min(d, ny - d))
     far_x = sorted(range(1, nx), key=lambda d: -min(d, nx - d))
-    others = info.at[pl.ds(1, nz - 1)]
-    columns = sgu_v.at[:, pl.ds(0, nz - 1), 0, 0]
-    own = sgu_v.at[:, z, y, c]
-    for d in far_z:
-        send(SZ, own, own, in_r.at[SZ], z_peer(d), columns)
-    for d in far_z:
-        send(INFO, info.at[0], info.at[nz - d], in_r.at[INFO], z_peer(d), others)
-
     local["len"].wait()
     local["bias"].wait()
     for n in range(rows):
@@ -291,8 +281,12 @@
         at = slice(i * quarter, (i + 1) * quarter)
         att[i] = mm(heads_out, wo_v[:, at]).astype(BF16)
 
+    pl.semaphore_wait(barrier, len(peers))
     for d in far_x:
         send(AT, att.at[(x + d) % nx], att_in.at[d - 1], in_r.at[AT], x_peer(d), att_in)
+    others = info.at[pl.ds(1, nz - 1)]
+    for d in far_z:
+        send(INFO, info.at[0], info.at[nz - d], in_r.at[INFO], z_peer(d), others)
 
     local["tokq"].wait()
     total = tokq_v[...].astype(F32) + att[x].astype(F32)
@@ -352,23 +346,18 @@
     comb[0] = high
     comb[1] = (weigh - high.astype(F32)).astype(BF16)
 
-    arrived(columns, in_r.at[SZ])
-    three = sgu_v.at[:, :, pl.ds(0, 3), 0]
-    near = sgu_v.at[:, :, y, c]
-    for d in (1, ny - 1):
-        send(SY, near, near, in_r.at[SY], g_peer(2 * d), three)
-
     arrived(blocks, in_r.at[TZ])
     picked = mm(take[0:slots, :], tb[...].reshape(many, quarter))
     xs[x, 0] = picked[0:part].astype(BF16)
-    for g in [2 * d + k for d in far_y for k in range(2)] + [1]:
+    for g in [1] + [2 * d + k for d in reversed(far_y) for k in range(2)]:
         slot_out[g - 1] = picked[g * part : (g + 1) * part].astype(BF16)
         send(SL, slot_out.at[g - 1], xs.at[x, g_back(g)], sl_r.at[g_back(g)], g_peer(g), slot_out)
     order = [0, 1] + [2 * d + k for d in reversed(far_y) for k in range(2)]
     right, left = (x + 1) % nx, (x + nx - 1) % nx
     pairs = [order[i : i + 2] for i in range(0, groups, 2)]
-    direct = pairs[-1]
-    rightward = [s for at, s in enumerate(order) if at in RIGHT]
+    direct = sum(pairs[len(pairs) - SUM_DIRECT :], [])
+    gather_right = [s for at, s in enumerate(order) if at in GATHER_RIGHT]
+    sum_right = [s for at, s in enumerate(order) if at in SUM_RIGHT]
     chunks = xs.at[pl.ds(0, 3)]
 
     def rest(s):
@@ -376,14 +365,14 @@
 
     def gather_send(s):
         here = xs.at[x, s]
-        for d in far_x if s in direct else (1, nx - 1):
-            first = s not in direct and (d == 1) == (s in rightward)
+        for d in (1, nx - 1):
+            first = (d == 1) == (s in gather_right)
             send(XF, here, here, xf_r.at[s] if first else rest(s), x_peer(d), chunks)
 
     def gather_pass(s):
-        here = xs.at[left if s in rightward else right, s]
+        here = xs.at[left if s in gather_right else right, s]
         arrived(here, xf_r.at[s])
-        send(XF, here, here, rest(s), x_peer(1 if s in rightward else nx - 1), chunks)
+        send(XF, here, here, rest(s), x_peer(1 if s in gather_right else nx - 1), chunks)
 
     parts = ys.at[pl.ds(0, 3)]
 
@@ -392,12 +381,12 @@
             for d in far_x:
                 send(YX, ys.at[(x + d) % nx, s], ys_in.at[s, d - 1], yn_r.at[s], x_peer(d), parts)
             return
-        on, off = (1, nx - 1) if s in rightward else (nx - 1, 1)
+        on, off = (1, nx - 1) if s in sum_right else (nx - 1, 1)
         send(YX, ys.at[(x + 2) % nx, s], opp_in.at[s], yo_r.at[s], x_peer(on), parts)
         send(YX, ys.at[(x + off) % nx, s], ys_in.at[s, 0], yn_r.at[s], x_peer(off), parts)
 
     def sum_pass(s):
-        on = 1 if s in rightward else nx - 1
+        on = 1 if s in sum_right else nx - 1
         arrived(opp_in.at[s], yo_r.at[s])
         opp_out[s] = (ys[(x + on) % nx, s].astype(F32) + opp_in[s].astype(F32)).astype(BF16)
         send(YX, opp_out.at[s], ys_in.at[s, 1], yn_r.at[s], x_peer(on), parts)
@@ -414,8 +403,10 @@
             yy[s - 1] = total.astype(BF16)
             send(YG, yy.at[s - 1], ret.at[g_back(s)], in_r.at[YG], g_peer(s), yy)
 
-    def experts(some):
-        arrived(xs.at[0, pl.ds(0, 6 if some == direct else 4)], rest(some[0]))
+    def experts(*ready):
+        for pair in ready:
+            arrived(xs.at[0, pl.ds(0, 4)], rest(pair[0]))
+        some = sum(ready, [])
         pieces = [
             jnp.concatenate([xs[i, s].astype(F32) for s in some], axis=0) for i in range(nx)
         ]
@@ -438,6 +429,13 @@
     for name in ("eg", "eu", "ed"):
         local[name].wait()
 
+    local["sg"].wait()
+    local["su"].wait()
+    columns = sgu_v.at[:, pl.ds(0, nz - 1), 0, 0]
+    own = sgu_v.at[:, z, y, c]
+    for d in far_z:
+        send(SZ, own, own, in_r.at[SZ], z_peer(d), columns)
+
     gather_send(0)
     arrived(xs.at[x, 1], sl_r.at[1])
     gather_send(1)
@@ -450,27 +448,35 @@
     for s in pairs[1]:
         gather_pass(s)
     experts(pairs[0])
+    arrived(columns, in_r.at[SZ])
+    three = sgu_v.at[:, :, pl.ds(0, 3), 0]
+    near = sgu_v.at[:, :, y, c]
+    for d in (1, ny - 1):
+        send(SY, near, near, in_r.at[SY], g_peer(2 * d), three)
+    for s in order[4:]:
+        gather_pass(s)
+    experts(pairs[1])
+    for s in pairs[0]:
+        sum_pass(s)
+    experts(*pairs[2:])
     arrived(sgu_v.at[:, :, pl.ds(0, 2), 0], in_r.at[SY])
     mid = nz // 2
     low_half = sgu_v.at[:, pl.ds(0, mid), (y + ny - 1) % ny, c]
     high_half = sgu_v.at[:, pl.ds(mid, mid), (y + 1) % ny, c]
     send(SY, low_half, low_half, in_r.at[SC], g_peer(2), three)
     send(SY, high_half, high_half, in_r.at[SC], g_peer(2 * (ny - 1)), three)
-    for s in order[4:-2]:
-        gather_pass(s)
-    experts(pairs[1])
-    for s in pairs[0]:
-        sum_pass(s)
-    for pair in pairs[2:]:
-        experts(pair)
-    for s in order[2:-2]:
-        sum_pass(s)
-
+    for s in order[2:]:
+        if s not in direct:
+            sum_pass(s)
+
+    for s in order[:4] + direct:
+        sum_end(s)
     arrived(near, in_r.at[SC])
     half = sgu_v.at[:, :, :, c]
     send(SC, half, half, in_r.at[SH], g_peer(1), sgu_v.at[:, :, :, 0])
-    for s in order:
-        sum_end(s)
+    for s in order[4:]:
+        if s not in direct:
+            sum_end(s)
 
     arrived(att_in, in_r.at[RX])
     mine = [res16[i].astype(F32) for i in range(nx)]

time: 55.4 us -> 51.9 us (0.937); the launches traced: 54.3 us -> 51.8 us
  Pallas kernels: 52.5 us -> 49.9 us
    pallas_call x1, Pallas kernels: 52.5 us -> 49.9 us  [shards(): pl.pallas_call(functools.partial(kernel, (nz, ny, nx)), out_shape=(jax.Sh...]
where the time goes in v4:
time: 51.9 us; the launch traced here: 51.8 us
  Pallas kernels  49.9 us (96%)
  local copies, waits for them, and re-layouts  1.2 us (2%)
  between operations  0.65 us (1%)
    pallas_call x1, Pallas kernels, shards(): pl.pallas_call(functools.partial(kernel, (nz, ny, nx)), out_shape=(jax.Sh...  49.9 us
    unnamed x2, local copies, waits for them, and re-layouts  1.2 us

profile of v4, /device:TPU:2, one launch (start us, length us, event | category | flops | bytes accessed | tf_op | source)
XLA Modules:
  0.0 51.8 jit_solution(11198087114209092106)
XLA Ops:
  0.6 49.9 %shard_map.194 = (bf16[16,512]{1,0:T(8,128)(2,1)S(1)}, bf16[16,128]{1,0:T(8,128)(2,1)S(1)}) custom-call(bf16[16,2048]{1,0:T(8,128)(2,1)} %tokens.1, s32[16]{0:T(128)} %lengths.1, bf16[16,1024,128]{2,1,0:T(8,128)(2,1)} %cache.1, f32[1,2048]{1,0:T(1,128)} %bitcast.9, bf16[2048,256]{1,0:T(8,128)(2,1)} %query_weight.1, bf16[64,2048]{1,0:T(8,128)(2,1)} %bitcast.7, ...), custom_call_target="tpu_custom_call" | custom-call | tf_op jit(solution)/shard_map/pallas_call | solution.py:636
  50.6 0.6 %copy.23 = bf16[16,512]{1,0:T(8,128)(2,1)} copy(bf16[16,512]{1,0:T(8,128)(2,1)S(1)} %get-tuple-element.4) | data formatting | bytes 32768
  51.2 0.6 %copy.24 = bf16[16,128]{1,0:T(8,128)(2,1)} copy(bf16[16,128]{1,0:T(8,128)(2,1)S(1)} %get-tuple-element.5) | data formatting | bytes 8192

commit v5 on v4

--- a/solution.py
+++ b/solution.py
@@ -14,6 +14,7 @@
 GATHER_RIGHT = (1, 3, 5, 7)
 SUM_RIGHT = (0, 1, 4, 5)
 SUM_DIRECT = 1
+EARLY = 1
 F32 = jnp.float32
 BF16 = jnp.bfloat16
 MESH = pl.DeviceIdType.MESH
@@ -163,42 +164,47 @@
     own_q = pl.multiple_of(x * quarter, quarter)
     fetch("tok", tokens, tok_v)
     fetch("again", attn_gain, again_v)
-    fetch("wq", query_weight, wq_v)
-    fetch("wk", key_weight, wk_v)
-    fetch("wv", value_weight, wv_v)
     fetch("len", lengths, len_m)
     fetch("bias", stick_bias, bias_m)
     fetch("routes", routes, routes_v)
     fetch("rw", route_weights, rw_v)
+    deep = width // 4
+    for i in range(4):
+        fetch("wq%d" % i, query_weight.at[pl.ds(i * deep, deep)], wq_v.at[pl.ds(i * deep, deep)])
+    chunk = rows // 4
+
+    def fetch_cache(n):
+        for m in range(n * chunk, (n + 1) * chunk):
+            pltpu.make_async_copy(cache.at[m], cache_v.at[m], csem.at[n]).start()
+        at = pl.ds(n * chunk, chunk)
+        return pltpu.make_async_copy(cache.at[at], cache_v.at[at], csem.at[n])
+
+    cached = [fetch_cache(n) for n in range(EARLY)]
     barrier = pltpu.get_barrier_semaphore()
     for peer in peers:
         pl.semaphore_signal(barrier, inc=1, device_id=peer, device_id_type=MESH)
 
     local["tok"].wait()
     local["again"].wait()
-    chunk = rows // 4
-    cached = []
-    for n in range(4):
-        at = pl.ds(n * chunk, chunk)
-        copy = pltpu.make_async_copy(cache.at[at], cache_v.at[at], csem.at[n])
-        copy.start()
-        cached.append(copy)
+    for n in range(EARLY, 4):
+        cached.append(fetch_cache(n))
     tf = tok_v[...].astype(F32)
     normed = (
         tf * lax.rsqrt(jnp.mean(tf * tf, axis=-1, keepdims=True) + EPS) * again_v[...]
     ).astype(BF16)
-    local["wq"].wait()
-    q = mm(normed, wq_v[...]).astype(BF16).astype(F32)
-    local["wk"].wait()
-    local["wv"].wait()
-    new_kv[...] = jnp.concatenate(
-        [mm_nt(normed, wk_v[...]), mm_nt(normed, wv_v[...])], axis=1
-    ).astype(BF16)
+    q = jnp.zeros((rows, wq_v.shape[1]), F32)
+    for i in range(4):
+        local["wq%d" % i].wait()
+        at = slice(i * deep, (i + 1) * deep)
+        q = q + mm(normed[:, at], wq_v[at, :])
+    q = q.astype(BF16).astype(F32)
     for h in range(heads):
         qrow[pl.ds(h, rows, stride=heads), :] = jnp.concatenate(
             [q[:, h * HEAD_DIM : (h + 1) * HEAD_DIM], jnp.zeros((rows, HEAD_DIM), F32)], axis=1
         )
     fetch("wo", out_weight, wo_v)
+    fetch("wk", key_weight, wk_v)
+    fetch("wv", value_weight, wv_v)
     fetch("tokq", tokens.at[:, pl.ds(own_q, quarter)], tokq_v)
     fetch("fgain", ffn_gain, fgain_v)
     fetch("gv", gate_vector, gv_v)
@@ -208,19 +214,6 @@
     fetch("eu", expert_up.at[0], eu_v)
     fetch("sd", shared_down, sd_v)
     fetch("ed", expert_down.at[0], ed_v)
-    local["routes"].wait()
-    local["rw"].wait()
-    top = routes_v.shape[0]
-    info[0] = jnp.concatenate(
-        [
-            jnp.concatenate(
-                [routes_v[...].astype(F32), rw_v[...], jnp.zeros((top, 128 - 2 * rows), F32)], axis=1
-            ),
-            jnp.zeros((8 - top, 128), F32),
-        ],
-        axis=0,
-    )
-
     INFO, SZ, SY, SC, AT, RX, TZ, SL, XF, YX, YG, SH, ZB = range(13)
     LAST = SL
     posted = {}
@@ -281,6 +274,18 @@
         at = slice(i * quarter, (i + 1) * quarter)
         att[i] = mm(heads_out, wo_v[:, at]).astype(BF16)
 
+    local["routes"].wait()
+    local["rw"].wait()
+    top = routes_v.shape[0]
+    info[0] = jnp.concatenate(
+        [
+            jnp.concatenate(
+                [routes_v[...].astype(F32), rw_v[...], jnp.zeros((top, 128 - 2 * rows), F32)], axis=1
+            ),
+            jnp.zeros((8 - top, 128), F32),
+        ],
+        axis=0,
+    )
     pl.semaphore_wait(barrier, len(peers))
     for d in far_x:
         send(AT, att.at[(x + d) % nx], att_in.at[d - 1], in_r.at[AT], x_peer(d), att_in)
@@ -288,6 +293,11 @@
     for d in far_z:
         send(INFO, info.at[0], info.at[nz - d], in_r.at[INFO], z_peer(d), others)
 
+    local["wk"].wait()
+    local["wv"].wait()
+    new_kv[...] = jnp.concatenate(
+        [mm_nt(normed, wk_v[...]), mm_nt(normed, wv_v[...])], axis=1
+    ).astype(BF16)
     local["tokq"].wait()
     total = tokq_v[...].astype(F32) + att[x].astype(F32)
     arrived(att_in, in_r.at[AT])
@@ -363,6 +373,9 @@
     def rest(s):
         return xc_r.at[order.index(s) // 2]
 
+    def last(s):
+        return xc_r.at[(groups + order.index(s)) // 2]
+
     def gather_send(s):
         here = xs.at[x, s]
         for d in (1, nx - 1):
@@ -372,7 +385,7 @@
     def gather_pass(s):
         here = xs.at[left if s in gather_right else right, s]
         arrived(here, xf_r.at[s])
-        send(XF, here, here, rest(s), x_peer(1 if s in gather_right else nx - 1), chunks)
+        send(XF, here, here, last(s), x_peer(1 if s in gather_right else nx - 1), chunks)
 
     parts = ys.at[pl.ds(0, 3)]
 
@@ -404,18 +417,21 @@
             send(YG, yy.at[s - 1], ret.at[g_back(s)], in_r.at[YG], g_peer(s), yy)
 
     def experts(*ready):
-        for pair in ready:
-            arrived(xs.at[0, pl.ds(0, 4)], rest(pair[0]))
         some = sum(ready, [])
-        pieces = [
-            jnp.concatenate([xs[i, s].astype(F32) for s in some], axis=0) for i in range(nx)
-        ]
-        square = sum(jnp.sum(m * m, axis=-1, keepdims=True) for m in pieces)
+        square = gated = raised = 0.0
+        for d in (0, 1, nx - 1, 2):
+            if d in (1, 2):
+                for pair in ready:
+                    arrived(xs.at[0, pl.ds(0, 2)], last(pair[0]) if d == 2 else rest(pair[0]))
+            q = (x + d) % nx
+            at = pl.ds(pl.multiple_of(q * quarter, quarter), quarter)
+            piece = jnp.concatenate([xs[q, s].astype(F32) for s in some], axis=0)
+            square = square + jnp.sum(piece * piece, axis=-1, keepdims=True)
+            feats = (piece * fgain_v[:, at]).astype(BF16)
+            gated = gated + mm(feats, eg_v[at, :])
+            raised = raised + mm(feats, eu_v[at, :])
         scale = lax.rsqrt(square * (1.0 / width) + EPS)
-        feats = jnp.concatenate(
-            [(pieces[i] * scale * gain[i]).astype(BF16) for i in range(nx)], axis=1
-        )
-        hidden = (silu(mm(feats, eg_v[...])) * mm(feats, eu_v[...])).astype(BF16)
+        hidden = (silu(gated * scale) * (raised * scale)).astype(BF16)
         for i in range(nx):
             term = mm(hidden, ed_v[:, i * quarter : (i + 1) * quarter])
             for j, s in enumerate(some):
@@ -607,7 +623,7 @@
         vm((nz - 1, rows, quarter), BF16),
         vm((nx, rows, quarter), BF16),
         vm((nx - 1, rows, quarter), BF16),
-        dma((24,)),
+        dma((22,)),
         dma((4,)),
     ]
     scratch += [dma((13,)), dma((13,))] + [dma((groups,)) for _ in range(5)]

time: 51.9 us -> 50.9 us (0.981)
  Pallas kernels: 49.9 us -> 49 us
    pallas_call x1, Pallas kernels: 49.9 us -> 49 us  [shards(): pl.pallas_call(functools.partial(kernel, (nz, ny, nx)), out_shape=(jax.Sh...]
where the time goes in v5:
time: 50.9 us; the launch traced here: 50.8 us
  Pallas kernels  49 us (96%)
  local copies, waits for them, and re-layouts  1.2 us (2%)
  between operations  0.65 us (1%)
    pallas_call x1, Pallas kernels, shards(): pl.pallas_call(functools.partial(kernel, (nz, ny, nx)), out_shape=(jax.Sh...  49 us
    unnamed x2, local copies, waits for them, and re-layouts  1.2 us

profile of v5, /device:TPU:2, one launch (start us, length us, event | category | flops | bytes accessed | tf_op | source)
XLA Modules:
  0.0 50.8 jit_solution(3093005437596740158)
XLA Ops:
  0.6 49.0 %shard_map.194 = (bf16[16,512]{1,0:T(8,128)(2,1)S(1)}, bf16[16,128]{1,0:T(8,128)(2,1)S(1)}) custom-call(bf16[16,2048]{1,0:T(8,128)(2,1)} %tokens.1, s32[16]{0:T(128)} %lengths.1, bf16[16,1024,128]{2,1,0:T(8,128)(2,1)} %cache.1, f32[1,2048]{1,0:T(1,128)} %bitcast.9, bf16[2048,256]{1,0:T(8,128)(2,1)} %query_weight.1, bf16[64,2048]{1,0:T(8,128)(2,1)} %bitcast.7, ...), custom_call_target="tpu_custom_call" | custom-call | tf_op jit(solution)/shard_map/pallas_call | solution.py:652
  49.6 0.6 %copy.23 = bf16[16,512]{1,0:T(8,128)(2,1)} copy(bf16[16,512]{1,0:T(8,128)(2,1)S(1)} %get-tuple-element.4) | data formatting | bytes 32768
  50.2 0.6 %copy.24 = bf16[16,128]{1,0:T(8,128)(2,1)} copy(bf16[16,128]{1,0:T(8,128)(2,1)S(1)} %get-tuple-element.5) | data formatting | bytes 8192

commit v6 on v5

--- a/solution.py
+++ b/solution.py
@@ -12,8 +12,8 @@
 CAP = 3
 NY = 4
 GATHER_RIGHT = (1, 3, 5, 7)
-SUM_RIGHT = (0, 1, 4, 5)
-SUM_DIRECT = 1
+SUM_RIGHT = (0, 1)
+SUM_DIRECT = 2
 EARLY = 1
 F32 = jnp.float32
 BF16 = jnp.bfloat16
@@ -395,12 +395,12 @@
                 send(YX, ys.at[(x + d) % nx, s], ys_in.at[s, d - 1], yn_r.at[s], x_peer(d), parts)
             return
         on, off = (1, nx - 1) if s in sum_right else (nx - 1, 1)
-        send(YX, ys.at[(x + 2) % nx, s], opp_in.at[s], yo_r.at[s], x_peer(on), parts)
+        send(YX, ys.at[(x + 2) % nx, s], opp_in.at[s], yo_r.at[order.index(s)], x_peer(on), parts)
         send(YX, ys.at[(x + off) % nx, s], ys_in.at[s, 0], yn_r.at[s], x_peer(off), parts)
 
     def sum_pass(s):
         on = 1 if s in sum_right else nx - 1
-        arrived(opp_in.at[s], yo_r.at[s])
+        arrived(opp_in.at[s], yo_r.at[order.index(s)])
         opp_out[s] = (ys[(x + on) % nx, s].astype(F32) + opp_in[s].astype(F32)).astype(BF16)
         send(YX, opp_out.at[s], ys_in.at[s, 1], yn_r.at[s], x_peer(on), parts)
 
@@ -626,7 +626,7 @@
         dma((22,)),
         dma((4,)),
     ]
-    scratch += [dma((13,)), dma((13,))] + [dma((groups,)) for _ in range(5)]
+    scratch += [dma((13,)), dma((13,))] + [dma((n,)) for n in (groups, groups, groups - 2 * SUM_DIRECT, groups, groups)]
     spaces = [pltpu.HBM] * 19
     operands = (
         tokens,

time: 50.9 us -> 50.9 us (level); the launches traced: 50.8 us -> 50.2 us
  Pallas kernels: 49 us -> 48.3 us
    pallas_call x1, Pallas kernels: 49 us -> 48.3 us  [shards(): pl.pallas_call(functools.partial(kernel, (nz, ny, nx)), out_shape=(jax.Sh...]
where the time goes in v6:
time: 50.9 us; the launch traced here: 50.2 us
  Pallas kernels  48.3 us (95%)
  local copies, waits for them, and re-layouts  1.2 us (2%)
  between operations  0.65 us (1%)
    pallas_call x1, Pallas kernels, shards(): pl.pallas_call(functools.partial(kernel, (nz, ny, nx)), out_shape=(jax.Sh...  48.3 us
    unnamed x2, local copies, waits for them, and re-layouts  1.2 us

profile of v6, /device:TPU:2, one launch (start us, length us, event | category | flops | bytes accessed | tf_op | source)
XLA Modules:
  0.0 50.2 jit_solution(1275193239205562051)
XLA Ops:
  0.6 48.3 %shard_map.194 = (bf16[16,512]{1,0:T(8,128)(2,1)S(1)}, bf16[16,128]{1,0:T(8,128)(2,1)S(1)}) custom-call(bf16[16,2048]{1,0:T(8,128)(2,1)} %tokens.1, s32[16]{0:T(128)} %lengths.1, bf16[16,1024,128]{2,1,0:T(8,128)(2,1)} %cache.1, f32[1,2048]{1,0:T(1,128)} %bitcast.9, bf16[2048,256]{1,0:T(8,128)(2,1)} %query_weight.1, bf16[64,2048]{1,0:T(8,128)(2,1)} %bitcast.7, ...), custom_call_target="tpu_custom_call" | custom-call | tf_op jit(solution)/shard_map/pallas_call | solution.py:652
  49.0 0.6 %copy.23 = bf16[16,512]{1,0:T(8,128)(2,1)} copy(bf16[16,512]{1,0:T(8,128)(2,1)S(1)} %get-tuple-element.4) | data formatting | bytes 32768
  49.6 0.6 %copy.24 = bf16[16,128]{1,0:T(8,128)(2,1)} copy(bf16[16,128]{1,0:T(8,128)(2,1)S(1)} %get-tuple-element.5) | data formatting | bytes 8192
